TPU v7x, 512 devices: a whole 4x8x8 slice. The times are simulated.
512 devices in a mesh: kv: 64 (over z, y), tp: 8 (over x, core).
Axes of the slice: x: 4, y: 8, z: 8, core: 2. Of those that a mesh axis runs over, the one named last changes fastest.
Arguments:
- tokens: bfloat16 [128, 4096], P(None, 'kv'), may hold values from -16 to 16
- mix_gain: bfloat16 [4096], P('kv'), may hold values from 0.099609375 to 1.8984375
- ffn_gain: bfloat16 [4096], P('kv'), may hold values from 0.099609375 to 1.8984375
- w_query: bfloat16 [4096, 2048], P('kv', 'tp'), may hold values from -0.09375 to 0.09375
- w_key: bfloat16 [4096, 2048], P('kv', 'tp'), may hold values from -0.09375 to 0.09375
- w_value: bfloat16 [4096, 4096], P('kv', 'tp'), may hold values from -0.09375 to 0.09375
- w_gate: bfloat16 [4096, 4096], P('kv', 'tp'), may hold values from -0.09375 to 0.09375
- w_decay: bfloat16 [4096, 2048], P('kv', 'tp'), may hold values from -0.375 to 0.375
- decay_bias: float32 [2048], P('tp'), may hold values from -7 to 4
- head_gain: bfloat16 [512], replicated, may hold values from 0.099609375 to 1.8984375
- w_output: bfloat16 [4096, 4096], P('tp', 'kv'), may hold values from -0.09375 to 0.09375
- w_ffgate: bfloat16 [4096, 11008], P('kv', 'tp'), may hold values from -0.09375 to 0.09375
- w_ffup: bfloat16 [4096, 11008], P('kv', 'tp'), may hold values from -0.09375 to 0.09375
- w_down: bfloat16 [11008, 4096], P('tp', 'kv'), may hold values from -0.0546875 to 0.0546875
- state: float32 [128, 8, 256, 512], P('kv', 'tp'), may hold values from -6 to 6
Outputs:
- mixed: bfloat16 [128, 4096], P(None, 'kv')
- new_state: float32 [128, 8, 256, 512], P('kv', 'tp')
All inputs are finite; a program needn't handle non-finite values.
Results may differ from a plain program's by a relative error of at most 0.015.
Values may be sent and summed in bfloat16 or wider, within the bound.
A program may use at most 64 MiB of HBM per device.

v0:
```python
import jax
import jax.numpy as jnp
from jax import lax
from jax.sharding import PartitionSpec as P

epsilon = 1e-06


def split_up(x, dim, devices):
    before, after = (x.shape[:dim], x.shape[dim + 1 :])
    return jnp.moveaxis(x.reshape(*before, devices, -1, *after), dim, 0)


def summed_on_arrival(x, axis, dim):
    devices = lax.axis_size(axis)
    blocks = lax.all_to_all(split_up(x, dim, devices), axis, 0, 0, tiled=True)
    return jnp.sum(blocks.astype(jnp.float32), axis=0)


def in_one_piece(arrays, axis, dim, along):
    columns = [a.reshape(*a.shape[:along], -1) for a in arrays]
    both = jnp.concatenate(columns, axis=along)
    filled, at, gathered = (summed_on_arrival(both, axis, dim), 0, [])
    for a, column in zip(arrays, columns):
        section = filled[..., at : at + column.shape[along]]
        gathered.append(section.reshape(*section.shape[:along], *a.shape[along:]))
        at += column.shape[along]
    return tuple(gathered)


def joined_along(blocks, dim):
    shape = list(blocks.shape[1:])
    shape[dim] *= blocks.shape[0]
    return jnp.moveaxis(blocks, 0, dim).reshape(shape)


def sent_to_all(x, axis):
    devices = lax.axis_size(axis)
    return lax.all_to_all(jnp.broadcast_to(x[None], (devices, *x.shape)), axis, 0, 0, tiled=True)


def collect(x, axis, dim):
    return joined_along(sent_to_all(x, axis), dim)


def over_copies(x, axis):
    everything = sent_to_all(x, axis)
    return jnp.sum(everything.astype(jnp.float32), axis=0)


def local(
    tokens,
    mix_gain,
    ffn_gain,
    w_query,
    w_key,
    w_value,
    w_gate,
    w_decay,
    decay_bias,
    head_gain,
    w_output,
    w_ffgate,
    w_ffup,
    w_down,
    state,
):
    own_rows = state.shape[0]
    local_heads = state.shape[1]
    key_dim = state.shape[2]
    val_dim = state.shape[3]
    model_width = tokens.shape[1] * lax.axis_size("kv")
    token_f32 = tokens.astype(jnp.float32)
    row_squares = jnp.sum(token_f32 * token_f32, axis=1)
    mix_in = (token_f32 * mix_gain.astype(jnp.float32)).astype(jnp.bfloat16)
    query_part = jnp.dot(mix_in, w_query, preferred_element_type=jnp.float32)
    key_part = jnp.dot(mix_in, w_key, preferred_element_type=jnp.float32)
    value_part = jnp.dot(mix_in, w_value, preferred_element_type=jnp.float32)
    gate_part = jnp.dot(mix_in, w_gate, preferred_element_type=jnp.float32)
    decay_part = jnp.dot(mix_in, w_decay, preferred_element_type=jnp.float32)
    query_sum, key_sum, value_sum, gate_sum, decay_sum, own_squares = in_one_piece(
        (
            query_part.astype(jnp.bfloat16),
            key_part.astype(jnp.bfloat16),
            value_part.astype(jnp.bfloat16),
            gate_part.astype(jnp.bfloat16),
            decay_part.astype(jnp.bfloat16),
            row_squares.astype(jnp.bfloat16),
        ),
        "kv",
        0,
        1,
    )
    mix_rms = lax.rsqrt(own_squares / model_width + epsilon)[:, None]
    queries = (query_sum * mix_rms).reshape(own_rows, local_heads, key_dim) * key_dim ** (-0.5)
    key_rows = (key_sum * mix_rms).reshape(own_rows, local_heads, key_dim)
    value_rows = (value_sum * mix_rms).reshape(own_rows, local_heads, val_dim)
    gate_rows = (gate_sum * mix_rms).reshape(own_rows, local_heads, val_dim)
    decay_rows = (decay_sum * mix_rms + decay_bias).reshape(own_rows, local_heads, key_dim)
    log_decay = jax.nn.log_sigmoid(decay_rows) / 16.0
    new_state = (
        jnp.exp(log_decay)[..., None] * state + key_rows[..., :, None] * value_rows[..., None, :]
    )
    attended = jnp.einsum("bhk,bhkv->bhv", queries, new_state, precision=lax.Precision.HIGHEST)
    attended = attended * lax.rsqrt(
        jnp.sum(attended * attended, axis=2, keepdims=True) / val_dim + epsilon
    )
    head_out = (
        (attended * head_gain.astype(jnp.float32) * jax.nn.silu(gate_rows))
        .reshape(own_rows, local_heads * val_dim)
        .astype(jnp.bfloat16)
    )
    head_partial = jnp.dot(collect(head_out, "kv", 0), w_output, preferred_element_type=jnp.float32)
    attn_out = over_copies(head_partial.astype(jnp.bfloat16), "tp").astype(jnp.float32)
    residual_mid = (token_f32 + attn_out).astype(jnp.bfloat16)
    mid_f32 = residual_mid.astype(jnp.float32)
    mid_squares = jnp.sum(mid_f32 * mid_f32, axis=1)
    ffn_in = (mid_f32 * ffn_gain.astype(jnp.float32)).astype(jnp.bfloat16)
    ffgate_part = jnp.dot(ffn_in, w_ffgate, preferred_element_type=jnp.float32)
    ffup_part = jnp.dot(ffn_in, w_ffup, preferred_element_type=jnp.float32)
    ffgate_sum, ffup_sum, square_sum = in_one_piece(
        (
            ffgate_part.astype(jnp.bfloat16),
            ffup_part.astype(jnp.bfloat16),
            mid_squares.astype(jnp.bfloat16),
        ),
        "kv",
        0,
        1,
    )
    ffn_rms = lax.rsqrt(square_sum / model_width + epsilon)[:, None]
    hidden = (jax.nn.silu(ffgate_sum * ffn_rms) * (ffup_sum * ffn_rms)).astype(jnp.bfloat16)
    down_part = jnp.dot(collect(hidden, "kv", 0), w_down, preferred_element_type=jnp.float32)
    ffn_out = over_copies(down_part.astype(jnp.bfloat16), "tp").astype(jnp.float32)
    mixed = (mid_f32 + ffn_out).astype(jnp.bfloat16)
    return (mixed, new_state)


def solution(mesh):
    in_specs = (
        P(None, "kv"),
        P("kv"),
        P("kv"),
        P("kv", "tp"),
        P("kv", "tp"),
        P("kv", "tp"),
        P("kv", "tp"),
        P("kv", "tp"),
        P("tp"),
        P(),
        P("tp", "kv"),
        P("kv", "tp"),
        P("kv", "tp"),
        P("tp", "kv"),
        P("kv", "tp", None, None),
    )
    out_specs = (P(None, "kv"), P("kv", "tp", None, None))
    return jax.shard_map(local, mesh=mesh, in_specs=in_specs, out_specs=out_specs, check_vma=False)
```

profile of v0, /device:TPU:1, one launch (start us, length us, event | category | flops | bytes accessed | tf_op | source)
XLA Modules:
  0.0 142.9 jit_solution(15754888790524407089)
XLA Ops:
  0.7 0.7 convert_element_type.103
  1.4 0.7 fusion.3
  2.3 1.0 convolution_convert_fusion.5
  3.4 1.0 convolution_convert_fusion.4
  4.5 1.0 convolution_convert_fusion.6
  5.6 1.1 convolution_convert_fusion.3
  6.8 0.3 convolution_convert_fusion.2
  7.2 0.7 constant_dynamic-update-slice_fusion.5
  7.9 0.7 constant_dynamic-update-slice_fusion.4
  8.5 0.7 constant_dynamic-update-slice_fusion.3
  9.3 0.7 constant_dynamic-update-slice_fusion.2
  10.0 0.7 constant_dynamic-update-slice_fusion.1
  10.7 0.6 constant_dynamic-update-slice_fusion
  11.4 17.1 %all-to-all-start = ((bf16[64,2,1793]{2,1,0:T(2,128)(2,1)}), bf16[64,2,1793]{2,1,0:T(2,128)(2,1)S(1)}, u32[]{:S(2)}, u32[]{:S(2)}) async-start(bf16[64,2,1793]{2,1,0:T(2,128)(2,1)} %constant_dynamic-update-slice_fusion), calls=%async_computation | async-start | bytes 983040 | tf_op jit(solution)/shard_map/all_to_all | solution.py:16
  28.5 16.7 %all-to-all-done = bf16[64,2,1793]{2,1,0:T(2,128)(2,1)S(1)} async-done(((bf16[64,2,1793]{2,1,0:T(2,128)(2,1)}), bf16[64,2,1793]{2,1,0:T(2,128)(2,1)S(1)}, u32[]{:S(2)}, u32[]{:S(2)}) %all-to-all-start) | async-done | bytes 459040 | tf_op jit(solution)/shard_map/all_to_all | solution.py:16
  45.3 0.4 convert_reduce_fusion.1
  46.2 0.6 fusion
  47.2 17.8 %all_to_all.30 = bf16[64,2,512]{2,1,0:T(2,128)(2,1)S(1)} all-to-all(bf16[64,2,512]{2,1,0:T(2,128)(2,1)S(1)} %broadcast_in_dim.8), channel_id=1, replica_groups=mesh['kv'=64,'tp'=8] {'kv'}, dimensions={0} | all-to-all | bytes 262144 | tf_op jit(solution)/shard_map/all_to_all | solution.py:39
  65.2 0.7 broadcast_in_dim.9
  65.9 7.2 %all-to-all-start.2 = ((bf16[8,128,64]{1,2,0:T(8,128)(2,1)}), bf16[8,128,64]{1,2,0:T(8,128)(2,1)S(1)}, u32[]{:S(2)}, u32[]{:S(2)}) async-start(bf16[8,128,64]{1,2,0:T(8,128)(2,1)} %broadcast_in_dim.9), calls=%async_computation.2 | async-start | bytes 262144 | tf_op jit(solution)/shard_map/all_to_all | solution.py:39
  73.1 5.2 %all-to-all-done.2 = bf16[8,128,64]{1,2,0:T(8,128)(2,1)S(1)} async-done(((bf16[8,128,64]{1,2,0:T(8,128)(2,1)}), bf16[8,128,64]{1,2,0:T(8,128)(2,1)S(1)}, u32[]{:S(2)}, u32[]{:S(2)}) %all-to-all-start.2) | async-done | bytes 131104 | tf_op jit(solution)/shard_map/all_to_all | solution.py:39
  78.4 0.2 convert_element_type.131
  78.6 0.3 convolution_convert_fusion
  79.3 0.3 convolution_convert_fusion.1
  80.0 3.4 %concatenate.30 = bf16[64,2,2753]{2,1,0:T(2,128)(2,1)S(1)} concatenate(bf16[64,2,1376]{2,1,0:T(2,128)(2,1)S(1)} %concatenate.28, bf16[64,2,1376]{2,1,0:T(2,128)(2,1)S(1)} %concatenate.29, bf16[64,2,1]{2,1,0:T(2,128)(2,1)S(1)} %convert_element_type.131), dimensions={2} | concatenate | bytes 1409536 | tf_op jit(solution)/shard_map/concatenate | solution.py:22
  83.4 24.6 %all_to_all.31 = bf16[64,2,2753]{2,1,0:T(2,128)(2,1)S(1)} all-to-all(bf16[64,2,2753]{2,1,0:T(2,128)(2,1)S(1)} %concatenate.30), channel_id=1, replica_groups=mesh['kv'=64,'tp'=8] {'kv'}, dimensions={0} | all-to-all | bytes 1409536 | tf_op jit(solution)/shard_map/all_to_all | solution.py:16
  108.0 0.6 convert_reduce_fusion
  109.1 20.8 %all_to_all.32 = bf16[64,2,1376]{2,1,0:T(2,128)(2,1)S(1)} all-to-all(bf16[64,2,1376]{2,1,0:T(2,128)(2,1)S(1)} %broadcast_in_dim.10), channel_id=1, replica_groups=mesh['kv'=64,'tp'=8] {'kv'}, dimensions={0} | all-to-all | bytes 704512 | tf_op jit(solution)/shard_map/all_to_all | solution.py:39
  130.0 0.3 reshape.123
  130.2 0.2 convolution_convert_fusion.8
  130.5 11.7 %all_to_all.33 = bf16[8,128,64]{1,2,0:T(8,128)(2,1)S(1)} all-to-all(bf16[8,128,64]{1,2,0:T(8,128)(2,1)S(1)} %broadcast_in_dim.11), channel_id=1, replica_groups=mesh['kv'=64,'tp'=8] {'tp'}, dimensions={0} | all-to-all | bytes 262144 | tf_op jit(solution)/shard_map/all_to_all | solution.py:39
  142.3 0.6 fusion.7
  (51 shorter events, 2.8 us)
Async XLA Ops:
  0.6 78.0 %copy-start = (bf16[64,1376]{1,0:T(8,128)(2,1)S(1)}, bf16[64,1376]{1,0:T(8,128)(2,1)}, u32[]{:S(2)}) copy-start(bf16[64,1376]{1,0:T(8,128)(2,1)} %param.27) | copy-start | bytes 528388
  0.6 6.2 %copy-start.3 = (bf16[128,64]{0,1:T(8,128)(2,1)S(1)}, bf16[128,64]{0,1:T(8,128)(2,1)}, u32[]{:S(2)}) copy-start(bf16[128,64]{0,1:T(8,128)(2,1)} %param.15) | copy-start | bytes 49156
  0.7 6.2 %copy-start.6 = (bf16[64,512]{1,0:T(8,128)(2,1)S(1)}, bf16[64,512]{1,0:T(8,128)(2,1)}, u32[]{:S(2)}) copy-start(bf16[64,512]{1,0:T(8,128)(2,1)} %param.21) | copy-start | bytes 196612
  7.2 21.3 %copy-start.8 = (bf16[512]{0:T(512)(128)(2,1)S(1)}, bf16[512]{0:T(512)(128)(2,1)}, u32[]{:S(2)}) copy-start(bf16[512]{0:T(512)(128)(2,1)} %param.24) | copy-start | bytes 3076
  8.5 37.3 %copy-start.9 = (f32[256]{0:T(256)S(1)}, f32[256]{0:T(256)}, u32[]{:S(2)}) copy-start(f32[256]{0:T(256)} %param.23) | copy-start | bytes 3076
  9.3 36.7 %copy-start.2 = (f32[2,1,256,512]{3,2,1,0:T(8,128)S(1)}, f32[2,1,256,512]{3,2,1,0:T(8,128)}, u32[]{:S(2)}) copy-start(f32[2,1,256,512]{3,2,1,0:T(8,128)} %param.29) | copy-start | bytes 3145732
  11.4 33.9 %all-to-all-start = ((bf16[64,2,1793]{2,1,0:T(2,128)(2,1)}), bf16[64,2,1793]{2,1,0:T(2,128)(2,1)S(1)}, u32[]{:S(2)}, u32[]{:S(2)}) async-start(bf16[64,2,1793]{2,1,0:T(2,128)(2,1)} %constant_dynamic-update-slice_fusion), calls=%async_computation | async-start | bytes 983040 | tf_op jit(solution)/shard_map/all_to_all | solution.py:16
  46.2 19.7 %copy-start.1 = (f32[2,1,256,512]{3,2,1,0:T(8,128)}, f32[2,1,256,512]{3,2,1,0:T(8,128)S(1)}, u32[]{:S(2)}) copy-start(f32[2,1,256,512]{3,2,1,0:T(8,128)S(1)} %multiply_add_fusion) | copy-start | bytes 3145732
  46.2 18.8 %copy-start.7 = (bf16[512,64]{0,1:T(8,128)(2,1)S(1)}, bf16[512,64]{0,1:T(8,128)(2,1)}, u32[]{:S(2)}) copy-start(bf16[512,64]{0,1:T(8,128)(2,1)} %param.25) | copy-start | bytes 196612
  46.2 26.9 %copy-start.10 = (bf16[64]{0:T(256)(128)(2,1)S(1)}, bf16[64]{0:T(256)(128)(2,1)}, u32[]{:S(2)}) copy-start(bf16[64]{0:T(256)(128)(2,1)} %param.17) | copy-start | bytes 388
  65.9 12.4 %all-to-all-start.2 = ((bf16[8,128,64]{1,2,0:T(8,128)(2,1)}), bf16[8,128,64]{1,2,0:T(8,128)(2,1)S(1)}, u32[]{:S(2)}, u32[]{:S(2)}) async-start(bf16[8,128,64]{1,2,0:T(8,128)(2,1)} %broadcast_in_dim.9), calls=%async_computation.2 | async-start | bytes 262144 | tf_op jit(solution)/shard_map/all_to_all | solution.py:39
  78.4 1.0 copy-start.4
  108.6 21.6 %copy-start.5 = (bf16[1376,64]{0,1:T(8,128)(2,1)S(1)}, bf16[1376,64]{0,1:T(8,128)(2,1)}, u32[]{:S(2)}) copy-start(bf16[1376,64]{0,1:T(8,128)(2,1)} %param.28) | copy-start | bytes 528388
where the time goes:
time: 144 us; the launch traced here: 143 us
  blocking collectives  75 us (52%)
  starting transfers between devices  24.3 us (17%)
  waiting for transfers between devices  22 us (15%)
  local copies, waits for them, and re-layouts  10.3 us (7%)
  matrix products  6.18 us (4%)
  other arithmetic  4.14 us (3%)
    all_to_all x3, blocking collectives, sent_to_all(): lax.all_to_all(jnp.broadcast_to(x[None], (devices, *x.shape)), axis, 0, 0...  50.4 us
    all_to_all x1, blocking collectives, summed_on_arrival(): blocks = lax.all_to_all(split_up(x, dim, devices), axis, 0, 0, tiled=True)  24.6 us
    all_to_all x1, starting transfers between devices, summed_on_arrival(): blocks = lax.all_to_all(split_up(x, dim, devices), axis, 0, 0, tiled=True)  17.1 us
    all_to_all x1, waiting for transfers between devices, summed_on_arrival(): blocks = lax.all_to_all(split_up(x, dim, devices), axis, 0, 0, tiled=True)  16.7 us
    all_to_all x1, starting transfers between devices, sent_to_all(): lax.all_to_all(jnp.broadcast_to(x[None], (devices, *x.shape)), axis, 0, 0...  7.21 us
    all_to_all x1, waiting for transfers between devices, sent_to_all(): lax.all_to_all(jnp.broadcast_to(x[None], (devices, *x.shape)), axis, 0, 0...  5.23 us
    concatenate x9, local copies, waits for them, and re-layouts, in_one_piece(): both = jnp.concatenate(columns, axis=along)  4.54 us
    unnamed x27, local copies, waits for them, and re-layouts  3.58 us
  transfers between devices with their start and end apart: 2, of which 2 were waited for; matrix products, arithmetic and copies ran while one was open for 0% of the time, Pallas kernels for 0%

commit v1 on v0

v1 whole, which is shorter than its diff:
```python
import jax
import jax.numpy as jnp
from jax import lax
from jax.experimental import pallas as pl
from jax.experimental.pallas import tpu as pltpu
from jax.sharding import PartitionSpec as P

MESH = pl.DeviceIdType.MESH
EPS = 1e-06
F32 = jnp.float32
BF16 = jnp.bfloat16
RING = 8
FAR_FIRST = (4, 3, 5, 2, 6, 1, 7)
Z_UNITS = 6
Y_UNITS = 5
UNITS = Z_UNITS + Y_UNITS
SKEW = 3


def far(k):
    odd = k % 2
    return (4 + (k // 2) * (1 - odd) - ((k + 1) // 2) * odd + RING) % RING


def wait_bytes(ref, sem):
    pltpu.make_async_copy(ref, ref, sem).wait()


def silu(v):
    return v / (1.0 + jnp.exp(-v))


def dot(a, b):
    return jnp.dot(a, b, preferred_element_type=F32)


def square_row(x):
    squares = x * x
    high = squares.astype(BF16)
    low = (squares - high.astype(F32)).astype(BF16)
    ones = jnp.ones((8, x.shape[1]), BF16)
    dims = (((1,), (1,)), ((), ()))
    total = lax.dot_general(ones, high, dims, preferred_element_type=F32)
    total = total + lax.dot_general(ones, low, dims, preferred_element_type=F32)
    return total[0:1, :]


def column_of(row, first, count):
    lane = lax.broadcasted_iota(jnp.int32, (count, row.shape[1]), 1)
    place = lax.broadcasted_iota(jnp.int32, (count, row.shape[1]), 0) + first
    return jnp.sum(jnp.where(lane == place, row, 0.0), axis=1, keepdims=True)


def kernel(
    tokens_h, mix_gain_h, ffn_gain_h, wq_h, wk_h, wv_h, wg_h, wd_h, bias_h, head_gain_h,
    wo_h, wfg_h, wfu_h, wdn_h, state_h,
    mixed_o, state_o,
    tokens_v, mix_gain_v, ffn_gain_v, w1_v, w2_v, bias_v, head_gain_v, wo_v, wfg_v, wfu_v, wdn_v, state_v,
    woa_v, wob_v, wgu_v, wda_v, wdb_v,
    az_s, az_r, ay_s, ay_r, az2_s, az2_r, ay2_s, ay2_r, ass_s, ass_r, ass2_s, ass2_r,
    b_s, b_r, c_s, c_r,
    dz_s, dz_r, dy_s, dy_r, dz2_s, dz2_r, dy2_s, dy2_r, dss_s, dss_r, dss2_s, dss2_r,
    e_s, e_r, f_s, f_r,
    in_sem, out_sem, send_sem, recv_sem,
):
    kv = lax.axis_index("kv")
    tp = lax.axis_index("tp")
    z = kv // RING
    y = kv % RING

    def at_z(d):
        return {"kv": ((z + d) % RING) * RING + y, "tp": tp}

    def at_y(d):
        return {"kv": z * RING + (y + d) % RING, "tp": tp}

    def at_tp(d):
        return {"kv": kv, "tp": (tp + d) % 8}

    barrier = pltpu.get_barrier_semaphore()
    for d in FAR_FIRST:
        for peer in (at_z(d), at_y(d), at_tp(d)):
            pl.semaphore_signal(barrier, inc=1, device_id=peer, device_id_type=MESH)

    def send(src, dst, slot, peer):
        pltpu.make_async_remote_copy(
            src_ref=src, dst_ref=dst, send_sem=send_sem.at[slot], recv_sem=recv_sem.at[slot],
            device_id=peer, device_id_type=MESH,
        ).start()

    loads = [
        (tokens_h, tokens_v), (mix_gain_h, mix_gain_v),
        (wq_h, w1_v.at[:, 0:256]), (wk_h, w1_v.at[:, 256:512]), (wd_h, w1_v.at[:, 512:768]),
        (wv_h.at[:, 0:128], w1_v.at[:, 768:896]), (wv_h.at[:, 128:512], w2_v.at[:, 0:384]),
        (wg_h, w2_v.at[:, 384:896]),
        (state_h, state_v), (bias_h, bias_v), (head_gain_h, head_gain_v), (ffn_gain_h, ffn_gain_v),
        (wo_h, wo_v), (wfg_h, wfg_v), (wfu_h, wfu_v), (wdn_h, wdn_v),
    ]
    copies = [pltpu.make_async_copy(src, dst, in_sem.at[n]) for n, (src, dst) in enumerate(loads)]
    for copy in copies:
        copy.start()
    for copy in copies[:8]:
        copy.wait()

    token_f32 = tokens_v[...].astype(F32)
    mix_in = (token_f32 * mix_gain_v[...].astype(F32)).astype(BF16)
    ass_s[0] = square_row(token_f32)
    az_s[...] = dot(mix_in, w1_v[...]).astype(BF16).reshape(az_s.shape)
    row = lax.broadcasted_iota(jnp.int32, (128, 128), 0)
    col = lax.broadcasted_iota(jnp.int32, (128, 128), 1)
    source = 16 * ((row % 16) // 2) + 2 * (row // 16) + row % 2
    shuffle = jnp.where(col == source, 1.0, 0.0).astype(BF16)
    mix_by_y = dot(shuffle, mix_in).astype(BF16)
    ay_s[...] = dot(mix_by_y, w2_v[...]).astype(BF16).reshape(ay_s.shape)

    pl.semaphore_wait(barrier, 21)
    for n, d in enumerate(FAR_FIRST):
        send(az_s.at[(z + d) % RING], az_r.at[d - 1], 0, at_z(d))
        send(ay_s.at[(y + d) % RING], ay_r.at[d - 1], 1, at_y(d))
        send(ass_s.at[0], ass_r.at[d - 1], 2, at_z(d))

    for copy in copies[8:]:
        copy.wait()
    zeros = jnp.zeros((512, 64), BF16)
    woa_v[...] = jnp.concatenate([wo_v[...], zeros], axis=1)
    wob_v[...] = jnp.concatenate([zeros, wo_v[...]], axis=1)
    rows = wdn_v.shape[0]
    zeros = jnp.zeros((rows, 64), BF16)
    wda_v[pl.ds(0, rows)] = jnp.concatenate([wdn_v[...], zeros], axis=1)
    wdb_v[pl.ds(0, rows)] = jnp.concatenate([zeros, wdn_v[...]], axis=1)
    wda_v[pl.ds(rows, 128 * UNITS - rows)] = jnp.zeros((128 * UNITS - rows, 128), BF16)
    wdb_v[pl.ds(rows, 128 * UNITS - rows)] = jnp.zeros((128 * UNITS - rows, 128), BF16)
    for u in range(UNITS):
        for side, ref in enumerate((wfg_v, wfu_v)):
            at = 256 * u + 128 * side
            width = min(128, ref.shape[1] - 128 * u)
            part = ref[:, 128 * u : 128 * u + width]
            if width < 128:
                part = jnp.concatenate([part, jnp.zeros((64, 128 - width), BF16)], axis=1)
            wgu_v[:, at : at + 128] = part

    wait_bytes(az_r, recv_sem.at[0])
    by_z = az_s[z].astype(F32)
    for n in range(7):
        by_z = by_z + az_r[n].astype(F32)
    by_z = by_z.astype(BF16)
    for n in range(RING):
        az2_s[n] = by_z[2 * n : 2 * n + 2, :]
    wait_bytes(ass_r, recv_sem.at[2])
    ss = ass_s[0]
    for n in range(7):
        ss = ss + ass_r[n]
    ass2_s[0] = ss
    for d in FAR_FIRST:
        send(az2_s.at[(y + d) % RING], az2_r.at[d - 1], 3, at_y(d))
        send(ass2_s.at[0], ass2_r.at[d - 1], 5, at_y(d))
    wait_bytes(ay_r, recv_sem.at[1])
    by_y = ay_s[y].astype(F32)
    for n in range(7):
        by_y = by_y + ay_r[n].astype(F32)
    by_y = by_y.astype(BF16)
    for n in range(RING):
        ay2_s[n] = by_y[2 * n : 2 * n + 2, :]
    for d in FAR_FIRST:
        send(ay2_s.at[(z + d) % RING], ay2_r.at[d - 1], 4, at_z(d))

    wait_bytes(az2_r, recv_sem.at[3])
    wait_bytes(ay2_r, recv_sem.at[4])
    wait_bytes(ass2_r, recv_sem.at[5])
    left = az2_s[y].astype(F32)
    right = ay2_s[z].astype(F32)
    ss = ass2_s[0]
    for n in range(7):
        left = left + az2_r[n].astype(F32)
        right = right + ay2_r[n].astype(F32)
        ss = ss + ass2_r[n]
    mix_rms = lax.rsqrt(column_of(ss, 2 * kv, 2) / 4096.0 + EPS)
    left = left * mix_rms
    right = right * mix_rms
    queries = left[:, 0:256] * (256.0 ** -0.5)
    keys = left[:, 256:512]
    raw_decay = left[:, 512:768] + bias_v[...]
    log_decay = (jnp.minimum(raw_decay, 0.0) - jnp.log1p(jnp.exp(-jnp.abs(raw_decay)))) / 16.0
    decay = jnp.exp(log_decay)
    values = jnp.concatenate([left[:, 768:896], right[:, 0:384]], axis=1)
    gates = right[:, 384:896]
    columns = jnp.concatenate([decay, keys, queries, queries], axis=0).T
    outs = []
    for s in range(2):
        value = values[s : s + 1, :]
        total = jnp.zeros((8, 512), F32)
        for block in range(8):
            rows = slice(32 * block, 32 * block + 32)
            fresh = columns[rows, s : s + 1] * state_v[s, rows, :] + columns[rows, 2 + s : 3 + s] * value
            state_v[s, rows, :] = fresh
            weighted = columns[rows, 4 + s : 5 + s] * fresh
            total = total + weighted[0:8] + weighted[8:16] + weighted[16:24] + weighted[24:32]
        outs.append(jnp.sum(total, axis=0, keepdims=True))
    state_out = pltpu.make_async_copy(state_v, state_o, out_sem.at[0])
    state_out.start()
    attended = jnp.concatenate(outs, axis=0)
    attended = attended * lax.rsqrt(jnp.sum(attended * attended, axis=1, keepdims=True) / 512.0 + EPS)
    head_out = (attended * head_gain_v[...].astype(F32) * silu(gates)).astype(BF16)
    b_s[0] = head_out
    b_r[kv] = head_out

    def spread_b(k, carry):
        peer = ((z + far(k // RING)) % RING) * RING + (y + far(k % RING)) % RING
        send(b_s.at[0], b_r.at[kv], 6, {"kv": peer, "tp": tp})
        return carry

    lax.fori_loop(0, 63, spread_b, 0)
    wait_bytes(b_r.at[pl.ds(0, 63)], recv_sem.at[6])
    heads = b_r[...].reshape(128, 512)
    partial = (dot(heads[0:64], woa_v[...]) + dot(heads[64:128], wob_v[...])).astype(BF16)
    c_s[0] = partial
    c_r[tp] = partial
    for d in (4, 3, 5, 2, 6, 1, 7):
        send(c_s.at[0], c_r.at[tp], 7, at_tp(d))
    token_pack = jnp.concatenate([token_f32[0:64], token_f32[64:128]], axis=1)
    gain_pack = jnp.concatenate([ffn_gain_v[...], ffn_gain_v[...]], axis=1).astype(F32)
    wait_bytes(c_r.at[pl.ds(0, 7)], recv_sem.at[7])
    attn_out = c_r[0].astype(F32)
    for n in range(1, 8):
        attn_out = attn_out + c_r[n].astype(F32)
    mid = (token_pack + attn_out).astype(BF16).astype(F32)
    ffn_pack = (mid * gain_pack).astype(BF16)
    ffn_in = jnp.concatenate([ffn_pack[:, 0:64], ffn_pack[:, 64:128]], axis=0)
    dss_s[0] = square_row(jnp.concatenate([mid[:, 0:64], mid[:, 64:128]], axis=0))
    for u in range(UNITS):
        part = dot(ffn_in, wgu_v[:, 256 * u : 256 * u + 256]).astype(BF16)
        for n in range(RING):
            block = part[16 * n : 16 * n + 16, :]
            if u < Z_UNITS:
                dz_s[n, u] = block
            else:
                dy_s[(SKEW * n + u - Z_UNITS - 2) % RING, u - Z_UNITS] = block
        if u == Z_UNITS - 1:
            for d in FAR_FIRST:
                send(dz_s.at[(z + d) % RING], dz_r.at[d - 1], 8, at_z(d))
                send(dss_s.at[0], dss_r.at[d - 1], 10, at_z(d))
    for d in FAR_FIRST:
        send(dy_s.at[(y + d) % RING], dy_r.at[d - 1], 9, at_y(d))

    wait_bytes(dss_r, recv_sem.at[10])
    ss = dss_s[0]
    for n in range(7):
        ss = ss + dss_r[n]
    dss2_s[0] = ss
    for d in FAR_FIRST:
        send(dss2_s.at[0], dss2_r.at[d - 1], 13, at_y(d))
    wait_bytes(dy_r, recv_sem.at[9])
    for j in range(Y_UNITS):
        part = dy_s[y, j].astype(F32)
        for n in range(7):
            part = part + dy_r[n, j].astype(F32)
        dy2_s[j] = part.astype(BF16)
    for d in FAR_FIRST:
        j = (y - SKEW * (z + d) + 2 + 64) % RING

        @pl.when(j < Y_UNITS)
        def _(j=j, d=d):
            send(dy2_s.at[j], dy2_r.at[d - 1], 12, at_z(d))

    wait_bytes(dz_r, recv_sem.at[8])
    for i in range(Z_UNITS):
        part = dz_s[z, i].astype(F32)
        for n in range(7):
            part = part + dz_r[n, i].astype(F32)
        dz2_s[i] = part.astype(BF16)
    for d in FAR_FIRST:
        i = (y + d - SKEW * z + 64) % RING

        @pl.when(i < Z_UNITS)
        def _(i=i, d=d):
            send(dz2_s.at[i], dz2_r.at[d - 1], 11, at_y(d))

    place = (y - SKEW * z + 64) % RING
    place_y = (place + 2) % RING
    wait_bytes(dss2_r, recv_sem.at[13])
    ss = dss2_s[0]
    for n in range(7):
        ss = ss + dss2_r[n]
    ffn_rms = lax.rsqrt(column_of(ss, 16 * z, 16) / 4096.0 + EPS)

    def finish(total, unit, slot):
        total = total * ffn_rms
        hidden = (silu(total[:, 0:128]) * total[:, 128:256]).astype(BF16)
        e_s[slot] = hidden
        e_r[unit * RING + z] = hidden

        def spread(k, carry):
            peer = ((z + far(k // RING)) % RING) * RING + (y + far(k % RING)) % RING
            send(e_s.at[slot], e_r.at[unit * RING + z], 14, {"kv": peer, "tp": tp})
            return carry

        lax.fori_loop(0, 63, spread, 0)

    @pl.when(place_y < Y_UNITS)
    def _():
        wait_bytes(dy2_r, recv_sem.at[12])
        total = dy2_s[place_y].astype(F32)
        for n in range(7):
            total = total + dy2_r[n].astype(F32)
        finish(total, Z_UNITS + place_y, 1)

    @pl.when(place < Z_UNITS)
    def _():
        wait_bytes(dz2_r, recv_sem.at[11])
        total = dz2_s[place].astype(F32)
        for n in range(7):
            total = total + dz2_r[n].astype(F32)
        finish(total, place, 0)

    one_only = (place // Z_UNITS) + (place_y // Y_UNITS)

    @pl.when(one_only == 0)
    def _():
        wait_bytes(e_r.at[pl.ds(0, 86)], recv_sem.at[14])

    @pl.when(one_only != 0)
    def _():
        wait_bytes(e_r.at[pl.ds(0, 87)], recv_sem.at[14])

    partial = jnp.zeros((64, 128), F32)
    for u in range(UNITS):
        block = e_r[8 * u : 8 * u + 8].reshape(128, 128)
        rows = slice(128 * u, 128 * u + 128)
        partial = partial + dot(block[0:64], wda_v[rows, :]) + dot(block[64:128], wdb_v[rows, :])
    partial = partial.astype(BF16)
    f_s[0] = partial
    f_r[tp] = partial
    for d in (4, 3, 5, 2, 6, 1, 7):
        send(f_s.at[0], f_r.at[tp], 15, at_tp(d))
    wait_bytes(f_r.at[pl.ds(0, 7)], recv_sem.at[15])
    ffn_out = f_r[0].astype(F32)
    for n in range(1, 8):
        ffn_out = ffn_out + f_r[n].astype(F32)
    out = (mid + ffn_out).astype(BF16)
    mixed_o[...] = jnp.concatenate([out[:, 0:64], out[:, 64:128]], axis=0)

    state_out.wait()
    for slot, ref in enumerate((az_r, ay_r, ass_r, az2_r, ay2_r, ass2_r, b_r.at[pl.ds(0, 63)], c_r.at[pl.ds(0, 7)], dz_r, dy_r, dss_r)):
        wait_bytes(ref, send_sem.at[slot])
    wait_bytes(dss2_r, send_sem.at[13])
    one = pl.ds(0, 1)
    for d in FAR_FIRST:

        @pl.when((y - SKEW * (z + d) + 2 + 64) % RING < Y_UNITS)
        def _():
            wait_bytes(dy2_r.at[one], send_sem.at[12])

        @pl.when((y + d - SKEW * z + 64) % RING < Z_UNITS)
        def _():
            wait_bytes(dz2_r.at[one], send_sem.at[11])

    @pl.when(place < Z_UNITS)
    def _():
        wait_bytes(e_r.at[pl.ds(0, 63)], send_sem.at[14])

    @pl.when(place_y < Y_UNITS)
    def _():
        wait_bytes(e_r.at[pl.ds(0, 63)], send_sem.at[14])

    wait_bytes(f_r.at[pl.ds(0, 7)], send_sem.at[15])


def local(
    tokens, mix_gain, ffn_gain, w_query, w_key, w_value, w_gate, w_decay, decay_bias, head_gain,
    w_output, w_ffgate, w_ffup, w_down, state,
):
    hidden_units = w_ffgate.shape[1]
    state = state.reshape(2, 256, 512)
    V = pltpu.VMEM
    scratch = [
        V((128, 64), BF16), V((1, 64), BF16), V((1, 64), BF16), V((64, 896), BF16), V((64, 896), BF16),
        V((1, 256), F32), V((1, 512), BF16), V((512, 64), BF16), V((64, hidden_units), BF16),
        V((64, hidden_units), BF16), V((hidden_units, 64), BF16), V((2, 256, 512), F32),
        V((512, 128), BF16), V((512, 128), BF16), V((64, 256 * UNITS), BF16),
        V((128 * UNITS, 128), BF16), V((128 * UNITS, 128), BF16),
        V((8, 16, 896), BF16), V((7, 16, 896), BF16), V((8, 16, 896), BF16), V((7, 16, 896), BF16),
        V((8, 2, 896), BF16), V((7, 2, 896), BF16), V((8, 2, 896), BF16), V((7, 2, 896), BF16),
        V((1, 1, 128), F32), V((7, 1, 128), F32), V((1, 1, 128), F32), V((7, 1, 128), F32),
        V((1, 2, 512), BF16), V((64, 2, 512), BF16), V((1, 64, 128), BF16), V((8, 64, 128), BF16),
        V((8, Z_UNITS, 16, 256), BF16), V((7, Z_UNITS, 16, 256), BF16),
        V((8, Y_UNITS, 16, 256), BF16), V((7, Y_UNITS, 16, 256), BF16),
        V((Z_UNITS, 16, 256), BF16), V((7, 16, 256), BF16), V((Y_UNITS, 16, 256), BF16), V((7, 16, 256), BF16),
        V((1, 1, 128), F32), V((7, 1, 128), F32), V((1, 1, 128), F32), V((7, 1, 128), F32),
        V((2, 16, 128), BF16), V((8 * UNITS, 16, 128), BF16), V((1, 64, 128), BF16), V((8, 64, 128), BF16),
        pltpu.SemaphoreType.DMA((16,)), pltpu.SemaphoreType.DMA((1,)),
        pltpu.SemaphoreType.DMA((16,)), pltpu.SemaphoreType.DMA((16,)),
    ]
    mixed, new_state = pl.pallas_call(
        kernel,
        name="layer",
        out_shape=(
            jax.ShapeDtypeStruct((128, 64), BF16),
            jax.ShapeDtypeStruct((2, 256, 512), F32),
        ),
        in_specs=[pl.BlockSpec(memory_space=pl.ANY)] * 15,
        out_specs=(pl.BlockSpec(memory_space=pltpu.VMEM), pl.BlockSpec(memory_space=pl.ANY)),
        scratch_shapes=scratch,
        compiler_params=pltpu.CompilerParams(
            collective_id=0, has_side_effects=True, vmem_limit_bytes=60 * 2**20
        ),
    )(
        tokens, mix_gain.reshape(1, 64), ffn_gain.reshape(1, 64), w_query, w_key, w_value, w_gate, w_decay,
        decay_bias.reshape(1, 256), head_gain.reshape(1, 512), w_output, w_ffgate, w_ffup, w_down, state,
    )
    return (mixed, new_state.reshape(2, 1, 256, 512))


def solution(mesh):
    in_specs = (
        P(None, "kv"),
        P("kv"),
        P("kv"),
        P("kv", "tp"),
        P("kv", "tp"),
        P("kv", "tp"),
        P("kv", "tp"),
        P("kv", "tp"),
        P("tp"),
        P(),
        P("tp", "kv"),
        P("kv", "tp"),
        P("kv", "tp"),
        P("tp", "kv"),
        P("kv", "tp", None, None),
    )
    out_specs = (P(None, "kv"), P("kv", "tp", None, None))
    return jax.shard_map(local, mesh=mesh, in_specs=in_specs, out_specs=out_specs, check_vma=False)
```

time: 144 us -> 85.6 us (0.59)
  Pallas kernels: 0 us -> 75.7 us
  blocking collectives: 75 us -> 0 us
  starting transfers between devices: 24.3 us -> 0 us
  waiting for transfers between devices: 22 us -> 0 us
  matrix products: 6.18 us -> 0 us
  other arithmetic: 4.14 us -> 0 us
    pallas_call x0 -> x1, Pallas kernels: none -> 75.7 us  [local(): pl.pallas_call(kernel, name='layer', out_shape=(jax.ShapeDtypeStruct((128...]
    all_to_all x4 -> x0, blocking collectives: 75 us -> none  [the longest x3 50.4 us: sent_to_all(): lax.all_to_all(jnp.broadcast_to(x[None], (devices, *x.shape)), axis, 0, 0...]
    all_to_all x2 -> x0, starting transfers between devices: 24.3 us -> none  [the longest x1 17.1 us: summed_on_arrival(): blocks = lax.all_to_all(split_up(x, dim, devices), axis, 0, 0, tiled=True)]
    all_to_all x2 -> x0, waiting for transfers between devices: 22 us -> none  [the longest x1 16.7 us: summed_on_arrival(): blocks = lax.all_to_all(split_up(x, dim, devices), axis, 0, 0, tiled=True)]
    dot_general x10 -> x0, matrix products: 6.18 us -> none  [the longest x1 1.13 us: local(): value_part = jnp.dot(mix_in, w_value, preferred_element_type=jnp.float32)]
    concatenate x9 -> x0, local copies, waits for them, and re-layouts: 4.54 us -> none  [in_one_piece(): both = jnp.concatenate(columns, axis=along)]
    unnamed x27 -> x7, local copies, waits for them, and re-layouts: 3.58 us -> 7.64 us
    reduce_sum x7 -> x0, other arithmetic: 1.95 us -> none  [the longest x2 1.02 us: summed_on_arrival(): return jnp.sum(blocks.astype(jnp.float32), axis=0)]
  transfers between devices with their start and end apart: 2 -> 0, of which waited for: 2 -> 0; matrix products, arithmetic and copies ran while one was open for 0% -> 0% of each run, Pallas kernels for 0% -> 0%
where the time goes in v1:
time: 85.6 us; the launch traced here: 85.3 us
  Pallas kernels  75.7 us (88%)
  local copies, waits for them, and re-layouts  8.94 us (10%)
    pallas_call x1, Pallas kernels, local(): pl.pallas_call(kernel, name='layer', out_shape=(jax.ShapeDtypeStruct((128...  75.7 us
    unnamed x7, local copies, waits for them, and re-layouts  7.64 us

profile of v1, /device:TPU:1, one launch (start us, length us, event | category | flops | bytes accessed | tf_op | source)
XLA Modules:
  0.0 85.3 jit_solution(15403266868822001395)
XLA Ops:
  0.6 0.0 copy-start
  0.6 1.3 %reshape.25.head_gain_h = bf16[1,512]{1,0:T(2,128)(2,1)} reshape(bf16[512]{0:T(512)(128)(2,1)} %param.24) | data formatting | bytes 2048 | tf_op jit(solution)/shard_map/reshape | solution.py:408
  1.9 1.4 %copy.17.tokens_h = bf16[128,64]{1,0:T(8,128)(2,1)} copy(bf16[128,64]{0,1:T(8,128)(2,1)} %param.15) | data formatting | bytes 32768 | tf_op args[0]
  3.4 1.6 %copy.18.wo_h = bf16[512,64]{1,0:T(8,128)(2,1)} copy(bf16[512,64]{0,1:T(8,128)(2,1)} %param.25) | data formatting | bytes 131072 | tf_op args[10]
  5.0 0.0 copy-done
  5.0 0.9 %copy.19.wdn_h = bf16[1376,64]{1,0:T(8,128)(2,1)} copy(bf16[1376,64]{0,1:T(8,128)(2,1)S(1)} %copy-done) | data formatting | bytes 352256 | tf_op args[13]
  5.9 75.7 %layer.1 = (bf16[128,64]{1,0:T(8,128)(2,1)}, f32[2,256,512]{2,1,0:T(8,128)}) custom-call(bf16[128,64]{1,0:T(8,128)(2,1)} %copy.17.tokens_h, bf16[1,64]{1,0:T(2,128)(2,1)} %bitcast.10, bf16[1,64]{1,0:T(2,128)(2,1)} %bitcast.11, bf16[64,256]{1,0:T(8,128)(2,1)} %wq_h.1, bf16[64,256]{1,0:T(8,128)(2,1)} %wk_h.1, bf16[64,512]{1,0:T(8,128)(2,1)} %wv_h.1, ...), custom_call_target="tpu_custom_call" | custom-call | tf_op jit(solution)/shard_map/layer/pallas_call | solution.py:393
  81.5 1.4 %copy.20 = bf16[128,64]{0,1:T(8,128)(2,1)} copy(bf16[128,64]{1,0:T(8,128)(2,1)} %get-tuple-element.6) | data formatting | bytes 32768
  83.0 2.3 %copy.23 = f32[2,1,256,512]{3,2,1,0:T(8,128)} copy(f32[2,1,256,512]{3,2,1,0:T(8,128)} %bitcast.8) | data formatting | bytes 2097152
Async XLA Ops:
  0.6 4.3 %copy-start = (bf16[1376,64]{0,1:T(8,128)(2,1)S(1)}, bf16[1376,64]{0,1:T(8,128)(2,1)}, u32[]{:S(2)}) copy-start(bf16[1376,64]{0,1:T(8,128)(2,1)} %param.28) | copy-start | bytes 528388

commit v2 on v1

v2 whole, which is shorter than its diff:
```python
import jax
import jax.numpy as jnp
from jax import lax
from jax.experimental import pallas as pl
from jax.experimental.pallas import tpu as pltpu
from jax.sharding import PartitionSpec as P

MESH = pl.DeviceIdType.MESH
EPS = 1e-06
F32 = jnp.float32
BF16 = jnp.bfloat16
RING = 8
FAR_FIRST = (4, 3, 5, 2, 6, 1, 7)
UNITS = 11


def far(k):
    odd = k % 2
    return (4 + (k // 2) * (1 - odd) - ((k + 1) // 2) * odd + RING) % RING


def wait_bytes(ref, sem):
    pltpu.make_async_copy(ref, ref, sem).wait()


def silu(v):
    return v / (1.0 + jnp.exp(-v))


def dot(a, b):
    return jnp.dot(a, b, preferred_element_type=F32)


def dot_nt(a, b):
    return lax.dot_general(a, b, (((1,), (1,)), ((), ())), preferred_element_type=F32)


def square_row(x):
    squares = x * x
    high = squares.astype(BF16)
    low = (squares - high.astype(F32)).astype(BF16)
    ones = jnp.ones((8, x.shape[0]), BF16)
    return (dot(ones, high) + dot(ones, low))[0:1, :]


def column_of(row, first, count):
    lane = lax.broadcasted_iota(jnp.int32, (count, row.shape[1]), 1)
    place = lax.broadcasted_iota(jnp.int32, (count, row.shape[1]), 0) + first
    return jnp.sum(jnp.where(lane == place, row, 0.0), axis=1, keepdims=True)


def kernel(
    tokens_h, mix_gain_h, ffn_gain_h, wq_h, wk_h, wv_h, wg_h, wd_h, bias_h, head_gain_h,
    wo_h, wfg_h, wfu_h, wdn_h, state_h,
    mixed_o, rows_o,
    tokens_v, mix_gain_v, ffn_gain_v, w1_v, w2_v, bias_v, head_gain_v, wo_v, wfg_v, wfu_v, wdn_v, state_v,
    wgu_v, wlast_v,
    az_s, az_r, ay_s, ay_r, az2_s, az2_r, ay2_s, ay2_r, ass_s, ass_r, ass2_s, ass2_r,
    b_s, b_r, c_s, c_r,
    w_r, x_s, x_r, d_s, d_r, dss_s, dss_r, dss2_s, dss2_r,
    e_s, e_r, f_s, f_r,
    in_sem, send_sem, recv_sem,
):
    kv = lax.axis_index("kv")
    tp = lax.axis_index("tp")
    z = kv // RING
    y = kv % RING

    def at_z(d):
        return {"kv": ((z + d) % RING) * RING + y, "tp": tp}

    def at_y(d):
        return {"kv": z * RING + (y + d) % RING, "tp": tp}

    def at_tp(d):
        return {"kv": kv, "tp": (tp + d) % 8}

    def send(src, dst, slot, peer):
        pltpu.make_async_remote_copy(
            src_ref=src, dst_ref=dst, send_sem=send_sem.at[slot], recv_sem=recv_sem.at[slot],
            device_id=peer, device_id_type=MESH,
        ).start()

    loads = [
        (tokens_h, tokens_v), (mix_gain_h, mix_gain_v),
        (wq_h, w1_v.at[:, 0:256]), (wk_h, w1_v.at[:, 256:512]), (wd_h, w1_v.at[:, 512:768]),
        (wv_h.at[:, 0:128], w1_v.at[:, 768:896]), (wv_h.at[:, 128:512], w2_v.at[:, 0:384]),
        (wg_h, w2_v.at[:, 384:896]),
        (state_h, state_v), (bias_h, bias_v), (head_gain_h, head_gain_v), (ffn_gain_h, ffn_gain_v),
        (wo_h, wo_v), (wfg_h, wfg_v), (wfu_h, wfu_v), (wdn_h, wdn_v),
    ]
    copies = [pltpu.make_async_copy(src, dst, in_sem.at[n]) for n, (src, dst) in enumerate(loads)]
    for copy in copies:
        copy.start()
    barrier = pltpu.get_barrier_semaphore()
    for d in FAR_FIRST:
        for peer in (at_z(d), at_y(d), at_tp(d)):
            pl.semaphore_signal(barrier, inc=1, device_id=peer, device_id_type=MESH)

    for copy in copies[:6]:
        copy.wait()

    token_f32 = tokens_v[...].astype(F32)
    mix_t = (token_f32 * column_of(mix_gain_v[...].astype(F32), 0, 64)).astype(BF16)
    row = lax.broadcasted_iota(jnp.int32, (128, 128), 0)
    col = lax.broadcasted_iota(jnp.int32, (128, 128), 1)
    keep = jnp.where(col == row, 1.0, 0.0).astype(BF16)
    by_y = 16 * ((row % 16) // 2) + 2 * (row // 16) + row % 2
    shuffle = jnp.where(col == by_y, 1.0, 0.0).astype(BF16)
    mix_in = dot_nt(keep, mix_t).astype(BF16)
    az_s[...] = dot(mix_in, w1_v[...]).astype(BF16).reshape(az_s.shape)
    ass_s[0] = square_row(token_f32)

    pl.semaphore_wait(barrier, 21)
    for d in FAR_FIRST:
        send(az_s.at[(z + d) % RING], az_r.at[d - 1], 0, at_z(d))
    for copy in copies[6:8]:
        copy.wait()
    mix_by_y = dot_nt(shuffle, mix_t).astype(BF16)
    ay_s[...] = dot(mix_by_y, w2_v[...]).astype(BF16).reshape(ay_s.shape)
    for d in FAR_FIRST:
        send(ay_s.at[(y + d) % RING], ay_r.at[d - 1], 1, at_y(d))
    for d in FAR_FIRST:
        send(ass_s.at[0], ass_r.at[d - 1], 2, at_z(d))

    for copy in copies[8:]:
        copy.wait()
    last = wdn_v.shape[1] % 128
    wlast_v[...] = jnp.concatenate([wdn_v[:, 128 * UNITS - 128 :], jnp.zeros((64, 128 - last), BF16)], axis=1)
    for u in range(UNITS):
        for side, ref in enumerate((wfg_v, wfu_v)):
            width = min(128, ref.shape[1] - 128 * u)
            part = ref[:, 128 * u : 128 * u + width]
            if width < 128:
                part = jnp.concatenate([part, jnp.zeros((64, 128 - width), BF16)], axis=1)
            wgu_v[u, :, 128 * side : 128 * side + 128] = part
    w_r[0, y] = wgu_v[y]
    w_r[1, y] = wgu_v[8 + y // 3]

    wait_bytes(az_r, recv_sem.at[0])
    by_z = az_s[z].astype(F32)
    for n in range(7):
        by_z = by_z + az_r[n].astype(F32)
    by_z = by_z.astype(BF16)
    for n in range(RING):
        az2_s[n] = by_z[2 * n : 2 * n + 2, :]
    wait_bytes(ass_r, recv_sem.at[2])
    ss = ass_s[0]
    for n in range(7):
        ss = ss + ass_r[n]
    ass2_s[0] = ss
    for d in FAR_FIRST:
        send(az2_s.at[(y + d) % RING], az2_r.at[d - 1], 3, at_y(d))
        send(ass2_s.at[0], ass2_r.at[d - 1], 5, at_y(d))
    wait_bytes(ay_r, recv_sem.at[1])
    by_y = ay_s[y].astype(F32)
    for n in range(7):
        by_y = by_y + ay_r[n].astype(F32)
    by_y = by_y.astype(BF16)
    for n in range(RING):
        ay2_s[n] = by_y[2 * n : 2 * n + 2, :]
    for d in FAR_FIRST:
        send(ay2_s.at[(z + d) % RING], ay2_r.at[d - 1], 4, at_z(d))
    for d in FAR_FIRST:
        send(wgu_v.at[(y + d) % RING], w_r.at[0, y], 8, at_y(d))

    wait_bytes(az2_r, recv_sem.at[3])
    wait_bytes(ay2_r, recv_sem.at[4])
    wait_bytes(ass2_r, recv_sem.at[5])
    left = az2_s[y].astype(F32)
    right = ay2_s[z].astype(F32)
    ss = ass2_s[0]
    for n in range(7):
        left = left + az2_r[n].astype(F32)
        right = right + ay2_r[n].astype(F32)
        ss = ss + ass2_r[n]
    mix_rms = lax.rsqrt(column_of(ss, 2 * kv, 2) / 4096.0 + EPS)
    left = left * mix_rms
    right = right * mix_rms
    queries = left[:, 0:256] * (256.0 ** -0.5)
    keys = left[:, 256:512]
    raw_decay = left[:, 512:768] + bias_v[...]
    log_decay = (jnp.minimum(raw_decay, 0.0) - jnp.log1p(jnp.exp(-jnp.abs(raw_decay)))) / 16.0
    decay = jnp.exp(log_decay)
    values = jnp.concatenate([left[:, 768:896], right[:, 0:384]], axis=1)
    gates = right[:, 384:896]
    rows_o[:, 0:256] = decay
    rows_o[:, 256:512] = keys
    rows_o[:, 512:1024] = values
    columns = jnp.concatenate([decay, keys, queries, queries], axis=0).T
    outs = []
    for s in range(2):
        value = values[s : s + 1, :]
        total = jnp.zeros((8, 512), F32)
        for block in range(8):
            rows = slice(32 * block, 32 * block + 32)
            fresh = columns[rows, s : s + 1] * state_v[s, rows, :] + columns[rows, 2 + s : 3 + s] * value
            weighted = columns[rows, 4 + s : 5 + s] * fresh
            total = total + weighted[0:8] + weighted[8:16] + weighted[16:24] + weighted[24:32]
        outs.append(jnp.sum(total, axis=0, keepdims=True))
    attended = jnp.concatenate(outs, axis=0)
    attended = attended * lax.rsqrt(jnp.sum(attended * attended, axis=1, keepdims=True) / 512.0 + EPS)
    head_out = (attended * head_gain_v[...].astype(F32)[None, :] * silu(gates)).astype(BF16)
    b_s[0] = head_out
    b_r[kv] = head_out

    def spread_b(k, carry):
        peer = ((z + far(k // RING)) % RING) * RING + (y + far(k % RING)) % RING
        send(b_s.at[0], b_r.at[kv], 6, {"kv": peer, "tp": tp})
        return carry

    lax.fori_loop(0, 63, spread_b, 0)
    wait_bytes(b_r.at[pl.ds(0, 63)], recv_sem.at[6])
    heads = b_r[...].reshape(128, 512)
    partial = dot_nt(wo_v[...], heads).astype(BF16)
    c_s[0] = partial
    c_r[tp] = partial
    for d in (4, 3, 5, 2, 6, 1, 7):
        send(c_s.at[0], c_r.at[tp], 7, at_tp(d))
    for d in FAR_FIRST:

        @pl.when((y + d) % RING % 3 == 0)
        def _(d=d):
            send(wgu_v.at[8 + (y + d) % RING // 3], w_r.at[1, y], 9, at_y(d))

    gain_column = column_of(ffn_gain_v[...].astype(F32), 0, 64)
    wait_bytes(c_r.at[pl.ds(0, 7)], recv_sem.at[7])
    attn_out = c_r[0].astype(F32)
    for n in range(1, 8):
        attn_out = attn_out + c_r[n].astype(F32)
    mid = (token_f32 + attn_out).astype(BF16).astype(F32)
    ffn_in = (mid * gain_column).astype(BF16)
    x_s[0] = ffn_in
    x_r[y] = ffn_in
    for d in FAR_FIRST:
        send(x_s.at[0], x_r.at[y], 10, at_y(d))
    dss_s[0] = square_row(mid)
    for d in FAR_FIRST:
        send(dss_s.at[0], dss_r.at[d - 1], 11, at_y(d))

    second = y % 3 == 0
    wait_bytes(w_r.at[0, pl.ds(0, 7)], recv_sem.at[8])
    wait_bytes(x_r.at[pl.ds(0, 7)], recv_sem.at[10])
    rows_in = dot_nt(keep, x_r[...].reshape(512, 128)).astype(BF16)
    d_s[0] = dot(rows_in, w_r[0].reshape(512, 256)).astype(BF16).reshape(8, 16, 256)
    for d in FAR_FIRST:
        send(d_s.at[0, (z + d) % RING], d_r.at[0, d - 1], 12, at_z(d))

    @pl.when(second)
    def _():
        wait_bytes(w_r.at[1, pl.ds(0, 7)], recv_sem.at[9])
        d_s[1] = dot(rows_in, w_r[1].reshape(512, 256)).astype(BF16).reshape(8, 16, 256)
        for d in FAR_FIRST:
            send(d_s.at[1, (z + d) % RING], d_r.at[1, d - 1], 13, at_z(d))

    wait_bytes(dss_r, recv_sem.at[11])
    ss = dss_s[0]
    for n in range(7):
        ss = ss + dss_r[n]
    dss2_s[0] = ss
    for d in FAR_FIRST:
        send(dss2_s.at[0], dss2_r.at[d - 1], 14, at_z(d))
    wait_bytes(dss2_r, recv_sem.at[14])
    for n in range(7):
        ss = ss + dss2_r[n]
    ffn_rms = lax.rsqrt(column_of(ss, 16 * z, 16) / 4096.0 + EPS)

    def finish(unit, slot):
        wait_bytes(d_r.at[slot], recv_sem.at[12 + slot])
        total = d_s[slot, z].astype(F32)
        for n in range(7):
            total = total + d_r[slot, n].astype(F32)
        total = total * ffn_rms
        hidden = (silu(total[:, 0:128]) * total[:, 128:256]).astype(BF16)
        e_s[slot] = hidden
        e_r[unit * RING + z] = hidden

        def spread(k, carry):
            peer = ((z + far(k // RING)) % RING) * RING + (y + far(k % RING)) % RING
            send(e_s.at[slot], e_r.at[unit * RING + z], 15, {"kv": peer, "tp": tp})
            return carry

        lax.fori_loop(0, 63, spread, 0)

    @pl.when(second)
    def _():
        finish(8 + y // 3, 1)

    finish(y, 0)

    @pl.when(second)
    def _():
        wait_bytes(e_r.at[pl.ds(0, 86)], recv_sem.at[15])

    @pl.when(jnp.logical_not(second))
    def _():
        wait_bytes(e_r.at[pl.ds(0, 87)], recv_sem.at[15])

    hidden = jnp.concatenate([e_r[8 * u : 8 * u + 8].reshape(128, 128) for u in range(UNITS)], axis=1)
    weight = jnp.concatenate([wdn_v[:, 0 : 128 * UNITS - 128], wlast_v[...]], axis=1)
    partial = dot_nt(weight, hidden).astype(BF16)
    f_s[0] = partial
    f_r[tp] = partial
    for d in (4, 3, 5, 2, 6, 1, 7):
        send(f_s.at[0], f_r.at[tp], 16, at_tp(d))
    wait_bytes(f_r.at[pl.ds(0, 7)], recv_sem.at[16])
    ffn_out = f_r[0].astype(F32)
    for n in range(1, 8):
        ffn_out = ffn_out + f_r[n].astype(F32)
    mixed_o[...] = (mid + ffn_out).astype(BF16)

    seven = pl.ds(0, 7)
    drains = (
        az_r, ay_r, ass_r, az2_r, ay2_r, ass2_r, b_r.at[pl.ds(0, 63)], c_r.at[seven], w_r.at[0, seven], None,
        x_r.at[seven], dss_r, d_r.at[0], None, dss2_r, e_r.at[pl.ds(0, 63)], f_r.at[seven],
    )
    for slot, ref in enumerate(drains):
        if ref is not None:
            wait_bytes(ref, send_sem.at[slot])

    @pl.when(second)
    def _():
        wait_bytes(d_r.at[1], send_sem.at[13])
        wait_bytes(e_r.at[pl.ds(0, 63)], send_sem.at[15])

    for d in FAR_FIRST:

        @pl.when((y + d) % RING % 3 == 0)
        def _():
            wait_bytes(w_r.at[1, pl.ds(0, 1)], send_sem.at[9])


def local(
    tokens, mix_gain, ffn_gain, w_query, w_key, w_value, w_gate, w_decay, decay_bias, head_gain,
    w_output, w_ffgate, w_ffup, w_down, state,
):
    hidden_units = w_ffgate.shape[1]
    V = pltpu.VMEM
    scratch = [
        V((64, 128), BF16), V((1, 64), BF16), V((1, 64), BF16), V((64, 896), BF16), V((64, 896), BF16),
        V((1, 256), F32), V((512,), BF16), V((64, 512), BF16), V((64, hidden_units), BF16),
        V((64, hidden_units), BF16), V((64, hidden_units), BF16), V((2, 256, 512), F32),
        V((UNITS, 64, 256), BF16), V((64, 128), BF16),
        V((8, 16, 896), BF16), V((7, 16, 896), BF16), V((8, 16, 896), BF16), V((7, 16, 896), BF16),
        V((8, 2, 896), BF16), V((7, 2, 896), BF16), V((8, 2, 896), BF16), V((7, 2, 896), BF16),
        V((1, 1, 128), F32), V((7, 1, 128), F32), V((1, 1, 128), F32), V((7, 1, 128), F32),
        V((1, 2, 512), BF16), V((64, 2, 512), BF16), V((1, 64, 128), BF16), V((8, 64, 128), BF16),
        V((2, 8, 64, 256), BF16), V((1, 64, 128), BF16), V((8, 64, 128), BF16),
        V((2, 8, 16, 256), BF16), V((2, 7, 16, 256), BF16),
        V((1, 1, 128), F32), V((7, 1, 128), F32), V((1, 1, 128), F32), V((7, 1, 128), F32),
        V((2, 16, 128), BF16), V((8 * UNITS, 16, 128), BF16), V((1, 64, 128), BF16), V((8, 64, 128), BF16),
        pltpu.SemaphoreType.DMA((16,)),
        pltpu.SemaphoreType.DMA((17,)), pltpu.SemaphoreType.DMA((17,)),
    ]
    mixed, rows = pl.pallas_call(
        kernel,
        name="layer",
        out_shape=(
            jax.ShapeDtypeStruct((64, 128), BF16),
            jax.ShapeDtypeStruct((2, 1024), F32),
        ),
        in_specs=[pl.BlockSpec(memory_space=pltpu.HBM)] * 15,
        out_specs=[pl.BlockSpec(memory_space=pltpu.VMEM)] * 2,
        scratch_shapes=scratch,
        compiler_params=pltpu.CompilerParams(
            collective_id=0, has_side_effects=True, vmem_limit_bytes=64000000
        ),
    )(
        tokens.T, mix_gain.reshape(1, 64), ffn_gain.reshape(1, 64), w_query, w_key, w_value, w_gate, w_decay,
        decay_bias.reshape(1, 256), head_gain, w_output.T, w_ffgate, w_ffup, w_down.T, state.reshape(2, 256, 512),
    )
    decay, key, value = (rows[:, 0:256], rows[:, 256:512], rows[:, 512:1024])
    new_state = decay[:, None, :, None] * state + key[:, None, :, None] * value[:, None, None, :]
    return (mixed.T, new_state)


def solution(mesh):
    in_specs = (
        P(None, "kv"),
        P("kv"),
        P("kv"),
        P("kv", "tp"),
        P("kv", "tp"),
        P("kv", "tp"),
        P("kv", "tp"),
        P("kv", "tp"),
        P("tp"),
        P(),
        P("tp", "kv"),
        P("kv", "tp"),
        P("kv", "tp"),
        P("tp", "kv"),
        P("kv", "tp", None, None),
    )
    out_specs = (P(None, "kv"), P("kv", "tp", None, None))
    return jax.shard_map(local, mesh=mesh, in_specs=in_specs, out_specs=out_specs, check_vma=False)
```

time: 85.6 us -> 72.8 us (0.85)
  local copies, waits for them, and re-layouts: 8.94 us -> 1.36 us
  Pallas kernels: 75.7 us -> 69.3 us
  other arithmetic: 0 us -> 1.18 us
    unnamed x7, local copies, waits for them, and re-layouts: 7.64 us -> 0.62 us
    pallas_call x1, Pallas kernels: 75.7 us -> 69.3 us  [local(): pl.pallas_call(kernel, name='layer', out_shape=(jax.ShapeDtypeStruct((64,...]
    reshape x1 -> x0, local copies, waits for them, and re-layouts: 1.3 us -> none  [local(): head_gain.reshape(1, 512)]
    add x0 -> x1, other arithmetic: none -> 1.18 us  [local(): decay[:, None, :, None] * state]
where the time goes in v2:
time: 72.8 us; the launch traced here: 72.5 us
  Pallas kernels  69.3 us (95%)
  local copies, waits for them, and re-layouts  1.36 us (2%)
  other arithmetic  1.18 us (2%)
    pallas_call x1, Pallas kernels, local(): pl.pallas_call(kernel, name='layer', out_shape=(jax.ShapeDtypeStruct((64,...  69.3 us

profile of v2, /device:TPU:1, one launch (start us, length us, event | category | flops | bytes accessed | tf_op | source)
XLA Modules:
  0.0 72.5 jit_solution(15545237843341402679)
XLA Ops:
  0.6 0.0 copy-start
  0.6 69.3 %layer.1 = (bf16[64,128]{1,0:T(8,128)(2,1)}, f32[2,1024]{1,0:T(2,128)}) custom-call(bf16[64,128]{1,0:T(8,128)(2,1)} %bitcast.11, bf16[1,64]{1,0:T(2,128)(2,1)} %bitcast.14, bf16[1,64]{1,0:T(2,128)(2,1)} %bitcast.15, bf16[64,256]{1,0:T(8,128)(2,1)} %wq_h.1, bf16[64,256]{1,0:T(8,128)(2,1)} %wk_h.1, bf16[64,512]{1,0:T(8,128)(2,1)} %wv_h.1, ...), custom_call_target="tpu_custom_call" | custom-call | tf_op jit(solution)/shard_map/layer/pallas_call | solution.py:355
  70.0 0.0 copy-start.2
  70.0 0.7 %slice.11 = f32[2,512]{1,0:T(2,128)S(1)} slice(f32[2,1024]{1,0:T(2,128)} %get-tuple-element.5), slice={[0:2], [512:1024]} | slice | bytes 8192 | tf_op jit(solution)/shard_map/slice | solution.py:372
  70.7 0.0 copy-done.2
  70.7 0.0 copy-done
  70.7 0.0 copy-start.1
  70.8 1.2 %multiply_add_fusion = f32[2,1,256,512]{3,2,1,0:T(8,128)} fusion(f32[2,1,256,512]{3,2,1,0:T(8,128)S(1)} %copy-done, f32[2,512]{1,0:T(2,128)S(1)} %slice.11, f32[2,256]{1,0:T(2,128)S(1)} %get-tuple-element.7, f32[2,256]{1,0:T(2,128)S(1)} %get-tuple-element.6), kind=kLoop, calls=%fused_computation | loop fusion | flops 786432 | bytes 2105344 | tf_op jit(solution)/shard_map/add | solution.py:373
  71.9 0.0 copy-done.1
  71.9 0.6 copy.18
  (1 shorter events, 0.0 us)
Async XLA Ops:
  0.6 70.1 %copy-start = (f32[2,1,256,512]{3,2,1,0:T(8,128)S(1)}, f32[2,1,256,512]{3,2,1,0:T(8,128)}, u32[]{:S(2)}) copy-start(f32[2,1,256,512]{3,2,1,0:T(8,128)} %param.29) | copy-start | bytes 3145732
  70.0 0.8 %copy-start.2 = (f32[2,1024]{1,0:T(2,128)S(1)}, f32[2,1024]{1,0:T(2,128)}, u32[]{:S(2)}) copy-start(f32[2,1024]{1,0:T(2,128)} %get-tuple-element.5) | copy-start | bytes 24580
  70.7 1.2 %copy-start.1 = (bf16[64,128]{1,0:T(8,128)(2,1)S(1)}, bf16[64,128]{1,0:T(8,128)(2,1)}, u32[]{:S(2)}) copy-start(bf16[64,128]{1,0:T(8,128)(2,1)} %get-tuple-element.4) | copy-start | bytes 49156

commit v3 on v2

--- a/solution.py
+++ b/solution.py
@@ -52,13 +52,13 @@
 def kernel(
     tokens_h, mix_gain_h, ffn_gain_h, wq_h, wk_h, wv_h, wg_h, wd_h, bias_h, head_gain_h,
     wo_h, wfg_h, wfu_h, wdn_h, state_h,
-    mixed_o, rows_o,
+    mixed_o, decay_o, key_o, value_o,
     tokens_v, mix_gain_v, ffn_gain_v, w1_v, w2_v, bias_v, head_gain_v, wo_v, wfg_v, wfu_v, wdn_v, state_v,
-    wgu_v, wlast_v,
+    wgu_v, wdt_v,
     az_s, az_r, ay_s, ay_r, az2_s, az2_r, ay2_s, ay2_r, ass_s, ass_r, ass2_s, ass2_r,
     b_s, b_r, c_s, c_r,
     w_r, x_s, x_r, d_s, d_r, dss_s, dss_r, dss2_s, dss2_r,
-    e_s, e_r, f_s, f_r,
+    v_r, e_s, e_r, g_s, g_r, f_s, f_r,
     in_sem, send_sem, recv_sem,
 ):
     kv = lax.axis_index("kv")
@@ -125,17 +125,20 @@
 
     for copy in copies[8:]:
         copy.wait()
-    last = wdn_v.shape[1] % 128
-    wlast_v[...] = jnp.concatenate([wdn_v[:, 128 * UNITS - 128 :], jnp.zeros((64, 128 - last), BF16)], axis=1)
     for u in range(UNITS):
-        for side, ref in enumerate((wfg_v, wfu_v)):
+        for side, ref in enumerate((wfg_v, wfu_v, wdn_v)):
             width = min(128, ref.shape[1] - 128 * u)
             part = ref[:, 128 * u : 128 * u + width]
             if width < 128:
                 part = jnp.concatenate([part, jnp.zeros((64, 128 - width), BF16)], axis=1)
-            wgu_v[u, :, 128 * side : 128 * side + 128] = part
+            if side < 2:
+                wgu_v[u, :, 128 * side : 128 * side + 128] = part
+            else:
+                wdt_v[u] = part
     w_r[0, y] = wgu_v[y]
     w_r[1, y] = wgu_v[8 + y // 3]
+    v_r[0, y] = wdt_v[y]
+    v_r[1, y] = wdt_v[8 + y // 3]
 
     wait_bytes(az_r, recv_sem.at[0])
     by_z = az_s[z].astype(F32)
@@ -184,9 +187,9 @@
     decay = jnp.exp(log_decay)
     values = jnp.concatenate([left[:, 768:896], right[:, 0:384]], axis=1)
     gates = right[:, 384:896]
-    rows_o[:, 0:256] = decay
-    rows_o[:, 256:512] = keys
-    rows_o[:, 512:1024] = values
+    decay_o[...] = decay
+    key_o[...] = keys
+    value_o[...] = values
     columns = jnp.concatenate([decay, keys, queries, queries], axis=0).T
     outs = []
     for s in range(2):
@@ -253,6 +256,13 @@
         for d in FAR_FIRST:
             send(d_s.at[1, (z + d) % RING], d_r.at[1, d - 1], 13, at_z(d))
 
+    for d in FAR_FIRST:
+        send(wdt_v.at[(y + d) % RING], v_r.at[0, y], 18, at_y(d))
+
+        @pl.when((y + d) % RING % 3 == 0)
+        def _(d=d):
+            send(wdt_v.at[8 + (y + d) % RING // 3], v_r.at[1, y], 19, at_y(d))
+
     wait_bytes(dss_r, recv_sem.at[11])
     ss = dss_s[0]
     for n in range(7):
@@ -265,7 +275,7 @@
         ss = ss + dss2_r[n]
     ffn_rms = lax.rsqrt(column_of(ss, 16 * z, 16) / 4096.0 + EPS)
 
-    def finish(unit, slot):
+    def finish(slot):
         wait_bytes(d_r.at[slot], recv_sem.at[12 + slot])
         total = d_s[slot, z].astype(F32)
         for n in range(7):
@@ -273,37 +283,41 @@
         total = total * ffn_rms
         hidden = (silu(total[:, 0:128]) * total[:, 128:256]).astype(BF16)
         e_s[slot] = hidden
-        e_r[unit * RING + z] = hidden
-
-        def spread(k, carry):
-            peer = ((z + far(k // RING)) % RING) * RING + (y + far(k % RING)) % RING
-            send(e_s.at[slot], e_r.at[unit * RING + z], 15, {"kv": peer, "tp": tp})
-            return carry
-
-        lax.fori_loop(0, 63, spread, 0)
+        e_r[slot, z] = hidden
+        for d in FAR_FIRST:
+            send(e_s.at[slot], e_r.at[slot, z], 15 + slot, at_z(d))
 
     @pl.when(second)
     def _():
-        finish(8 + y // 3, 1)
-
-    finish(y, 0)
+        finish(1)
+
+    finish(0)
+
+    def down(slot):
+        wait_bytes(e_r.at[slot, pl.ds(0, 7)], recv_sem.at[15 + slot])
+        wait_bytes(v_r.at[slot, pl.ds(0, 7)], recv_sem.at[18 + slot])
+        return dot_nt(v_r[slot].reshape(512, 128), e_r[slot].reshape(128, 128))
 
     @pl.when(second)
     def _():
-        wait_bytes(e_r.at[pl.ds(0, 86)], recv_sem.at[15])
+        g_s[...] = (down(1) + down(0)).astype(BF16).reshape(8, 64, 128)
 
     @pl.when(jnp.logical_not(second))
     def _():
-        wait_bytes(e_r.at[pl.ds(0, 87)], recv_sem.at[15])
-
-    hidden = jnp.concatenate([e_r[8 * u : 8 * u + 8].reshape(128, 128) for u in range(UNITS)], axis=1)
-    weight = jnp.concatenate([wdn_v[:, 0 : 128 * UNITS - 128], wlast_v[...]], axis=1)
-    partial = dot_nt(weight, hidden).astype(BF16)
+        g_s[...] = down(0).astype(BF16).reshape(8, 64, 128)
+
+    for d in FAR_FIRST:
+        send(g_s.at[(y + d) % RING], g_r.at[d - 1], 20, at_y(d))
+    wait_bytes(g_r, recv_sem.at[20])
+    partial = g_s[y].astype(F32)
+    for n in range(7):
+        partial = partial + g_r[n].astype(F32)
+    partial = partial.astype(BF16)
     f_s[0] = partial
     f_r[tp] = partial
     for d in (4, 3, 5, 2, 6, 1, 7):
-        send(f_s.at[0], f_r.at[tp], 16, at_tp(d))
-    wait_bytes(f_r.at[pl.ds(0, 7)], recv_sem.at[16])
+        send(f_s.at[0], f_r.at[tp], 17, at_tp(d))
+    wait_bytes(f_r.at[pl.ds(0, 7)], recv_sem.at[17])
     ffn_out = f_r[0].astype(F32)
     for n in range(1, 8):
         ffn_out = ffn_out + f_r[n].astype(F32)
@@ -312,7 +326,8 @@
     seven = pl.ds(0, 7)
     drains = (
         az_r, ay_r, ass_r, az2_r, ay2_r, ass2_r, b_r.at[pl.ds(0, 63)], c_r.at[seven], w_r.at[0, seven], None,
-        x_r.at[seven], dss_r, d_r.at[0], None, dss2_r, e_r.at[pl.ds(0, 63)], f_r.at[seven],
+        x_r.at[seven], dss_r, d_r.at[0], None, dss2_r, e_r.at[0, seven], None, f_r.at[seven],
+        v_r.at[0, seven], None, g_r,
     )
     for slot, ref in enumerate(drains):
         if ref is not None:
@@ -321,13 +336,14 @@
     @pl.when(second)
     def _():
         wait_bytes(d_r.at[1], send_sem.at[13])
-        wait_bytes(e_r.at[pl.ds(0, 63)], send_sem.at[15])
+        wait_bytes(e_r.at[1, seven], send_sem.at[16])
 
     for d in FAR_FIRST:
 
         @pl.when((y + d) % RING % 3 == 0)
         def _():
             wait_bytes(w_r.at[1, pl.ds(0, 1)], send_sem.at[9])
+            wait_bytes(v_r.at[1, pl.ds(0, 1)], send_sem.at[19])
 
 
 def local(
@@ -340,7 +356,7 @@
         V((64, 128), BF16), V((1, 64), BF16), V((1, 64), BF16), V((64, 896), BF16), V((64, 896), BF16),
         V((1, 256), F32), V((512,), BF16), V((64, 512), BF16), V((64, hidden_units), BF16),
         V((64, hidden_units), BF16), V((64, hidden_units), BF16), V((2, 256, 512), F32),
-        V((UNITS, 64, 256), BF16), V((64, 128), BF16),
+        V((UNITS, 64, 256), BF16), V((UNITS, 64, 128), BF16),
         V((8, 16, 896), BF16), V((7, 16, 896), BF16), V((8, 16, 896), BF16), V((7, 16, 896), BF16),
         V((8, 2, 896), BF16), V((7, 2, 896), BF16), V((8, 2, 896), BF16), V((7, 2, 896), BF16),
         V((1, 1, 128), F32), V((7, 1, 128), F32), V((1, 1, 128), F32), V((7, 1, 128), F32),
@@ -348,28 +364,30 @@
         V((2, 8, 64, 256), BF16), V((1, 64, 128), BF16), V((8, 64, 128), BF16),
         V((2, 8, 16, 256), BF16), V((2, 7, 16, 256), BF16),
         V((1, 1, 128), F32), V((7, 1, 128), F32), V((1, 1, 128), F32), V((7, 1, 128), F32),
-        V((2, 16, 128), BF16), V((8 * UNITS, 16, 128), BF16), V((1, 64, 128), BF16), V((8, 64, 128), BF16),
+        V((2, 8, 64, 128), BF16), V((2, 16, 128), BF16), V((2, 8, 16, 128), BF16), V((8, 64, 128), BF16), V((7, 64, 128), BF16), V((1, 64, 128), BF16), V((8, 64, 128), BF16),
         pltpu.SemaphoreType.DMA((16,)),
-        pltpu.SemaphoreType.DMA((17,)), pltpu.SemaphoreType.DMA((17,)),
+        pltpu.SemaphoreType.DMA((21,)), pltpu.SemaphoreType.DMA((21,)),
     ]
-    mixed, rows = pl.pallas_call(
+    operands = (
+        tokens.T, mix_gain.reshape(1, 64), ffn_gain.reshape(1, 64), w_query, w_key, w_value, w_gate, w_decay,
+        decay_bias.reshape(1, 256), head_gain, w_output.T, w_ffgate, w_ffup, w_down.T, state.reshape(2, 256, 512),
+    )
+    mixed, decay, key, value = pl.pallas_call(
         kernel,
         name="layer",
         out_shape=(
             jax.ShapeDtypeStruct((64, 128), BF16),
-            jax.ShapeDtypeStruct((2, 1024), F32),
+            jax.ShapeDtypeStruct((2, 256), F32),
+            jax.ShapeDtypeStruct((2, 256), F32),
+            jax.ShapeDtypeStruct((2, 512), F32),
         ),
         in_specs=[pl.BlockSpec(memory_space=pltpu.HBM)] * 15,
-        out_specs=[pl.BlockSpec(memory_space=pltpu.VMEM)] * 2,
+        out_specs=[pl.BlockSpec(memory_space=pltpu.VMEM)] * 4,
         scratch_shapes=scratch,
         compiler_params=pltpu.CompilerParams(
-            collective_id=0, has_side_effects=True, vmem_limit_bytes=64000000
+            collective_id=0, has_side_effects=True, vmem_limit_bytes=40000000
         ),
-    )(
-        tokens.T, mix_gain.reshape(1, 64), ffn_gain.reshape(1, 64), w_query, w_key, w_value, w_gate, w_decay,
-        decay_bias.reshape(1, 256), head_gain, w_output.T, w_ffgate, w_ffup, w_down.T, state.reshape(2, 256, 512),
-    )
-    decay, key, value = (rows[:, 0:256], rows[:, 256:512], rows[:, 512:1024])
+    )(*[pltpu.with_memory_space_constraint(a, pltpu.HBM) for a in operands])
     new_state = decay[:, None, :, None] * state + key[:, None, :, None] * value[:, None, None, :]
     return (mixed.T, new_state)
 

time: 72.8 us -> 69.4 us (0.953)
  Pallas kernels: 69.3 us -> 66.8 us
  local copies, waits for them, and re-layouts: 1.36 us -> 0.61 us
    pallas_call x1, Pallas kernels: 69.3 us -> 66.8 us  [local(): pl.pallas_call(kernel, name='layer', out_shape=(jax.ShapeDtypeStruct((64,...]
    slice x2 -> x0, local copies, waits for them, and re-layouts: 0.74 us -> none  [local(): decay, key, value = (rows[:, 0:256], rows[:, 256:512], rows[:, 512:1024])]
where the time goes in v3:
time: 69.4 us; the launch traced here: 69.2 us
  Pallas kernels  66.8 us (96%)
  other arithmetic  1.18 us (2%)
    pallas_call x1, Pallas kernels, local(): pl.pallas_call(kernel, name='layer', out_shape=(jax.ShapeDtypeStruct((64,...  66.8 us

profile of v3, /device:TPU:1, one launch (start us, length us, event | category | flops | bytes accessed | tf_op | source)
XLA Modules:
  0.0 69.2 jit_solution(10114556237785741778)
XLA Ops:
  0.6 0.0 copy-start
  0.6 66.8 %layer.1 = (bf16[64,128]{1,0:T(8,128)(2,1)S(1)}, f32[2,256]{1,0:T(2,128)S(1)}, f32[2,256]{1,0:T(2,128)S(1)}, f32[2,512]{1,0:T(2,128)S(1)}) custom-call(bf16[64,128]{1,0:T(8,128)(2,1)} %bitcast.12, bf16[1,64]{1,0:T(2,128)(2,1)} %bitcast.14, bf16[1,64]{1,0:T(2,128)(2,1)} %bitcast.15, bf16[64,256]{1,0:T(8,128)(2,1)} %wq_h.1, bf16[64,256]{1,0:T(8,128)(2,1)} %wk_h.1, ...), custom_call_target="tpu_custom_call" | custom-call | tf_op jit(solution)/shard_map/layer/pallas_call | solution.py:375
  67.4 0.0 copy-done
  67.5 1.2 %multiply_add_fusion = f32[2,1,256,512]{3,2,1,0:T(8,128)} fusion(f32[2,1,256,512]{3,2,1,0:T(8,128)S(1)} %copy-done, f32[2,512]{1,0:T(2,128)S(1)} %get-tuple-element.9, f32[2,256]{1,0:T(2,128)S(1)} %get-tuple-element.8, f32[2,256]{1,0:T(2,128)S(1)} %get-tuple-element.7), kind=kLoop, calls=%fused_computation | loop fusion | flops 786432 | bytes 2105344 | tf_op jit(solution)/shard_map/add | solution.py:391
  68.6 0.6 copy.18
Async XLA Ops:
  0.6 66.8 %copy-start = (f32[2,1,256,512]{3,2,1,0:T(8,128)S(1)}, f32[2,1,256,512]{3,2,1,0:T(8,128)}, u32[]{:S(2)}) copy-start(f32[2,1,256,512]{3,2,1,0:T(8,128)} %param.29) | copy-start | bytes 3145732

commit v4 on v3

--- a/solution.py
+++ b/solution.py
@@ -12,6 +12,10 @@
 RING = 8
 FAR_FIRST = (4, 3, 5, 2, 6, 1, 7)
 UNITS = 11
+SPREAD = sorted(
+    ((dz, dy) for dz in range(RING) for dy in range(RING) if dz + dy > 0),
+    key=lambda t: -min(t[0], RING - t[0]) - min(t[1], RING - t[1]),
+)
 
 
 def far(k):
@@ -52,8 +56,8 @@
 def kernel(
     tokens_h, mix_gain_h, ffn_gain_h, wq_h, wk_h, wv_h, wg_h, wd_h, bias_h, head_gain_h,
     wo_h, wfg_h, wfu_h, wdn_h, state_h,
-    mixed_o, decay_o, key_o, value_o,
-    tokens_v, mix_gain_v, ffn_gain_v, w1_v, w2_v, bias_v, head_gain_v, wo_v, wfg_v, wfu_v, wdn_v, state_v,
+    mixed_o, state_v,
+    tokens_v, mix_gain_v, ffn_gain_v, w1_v, w2_v, bias_v, head_gain_v, wo_v, wfg_v, wfu_v, wdn_v,
     wgu_v, wdt_v,
     az_s, az_r, ay_s, ay_r, az2_s, az2_r, ay2_s, ay2_r, ass_s, ass_r, ass2_s, ass2_r,
     b_s, b_r, c_s, c_r,
@@ -111,14 +115,13 @@
     az_s[...] = dot(mix_in, w1_v[...]).astype(BF16).reshape(az_s.shape)
     ass_s[0] = square_row(token_f32)
 
-    pl.semaphore_wait(barrier, 21)
-    for d in FAR_FIRST:
-        send(az_s.at[(z + d) % RING], az_r.at[d - 1], 0, at_z(d))
     for copy in copies[6:8]:
         copy.wait()
     mix_by_y = dot_nt(shuffle, mix_t).astype(BF16)
     ay_s[...] = dot(mix_by_y, w2_v[...]).astype(BF16).reshape(ay_s.shape)
-    for d in FAR_FIRST:
+    pl.semaphore_wait(barrier, 21)
+    for d in FAR_FIRST:
+        send(az_s.at[(z + d) % RING], az_r.at[d - 1], 0, at_z(d))
         send(ay_s.at[(y + d) % RING], ay_r.at[d - 1], 1, at_y(d))
     for d in FAR_FIRST:
         send(ass_s.at[0], ass_r.at[d - 1], 2, at_z(d))
@@ -187,9 +190,6 @@
     decay = jnp.exp(log_decay)
     values = jnp.concatenate([left[:, 768:896], right[:, 0:384]], axis=1)
     gates = right[:, 384:896]
-    decay_o[...] = decay
-    key_o[...] = keys
-    value_o[...] = values
     columns = jnp.concatenate([decay, keys, queries, queries], axis=0).T
     outs = []
     for s in range(2):
@@ -198,6 +198,7 @@
         for block in range(8):
             rows = slice(32 * block, 32 * block + 32)
             fresh = columns[rows, s : s + 1] * state_v[s, rows, :] + columns[rows, 2 + s : 3 + s] * value
+            state_v[s, rows, :] = fresh
             weighted = columns[rows, 4 + s : 5 + s] * fresh
             total = total + weighted[0:8] + weighted[8:16] + weighted[16:24] + weighted[24:32]
         outs.append(jnp.sum(total, axis=0, keepdims=True))
@@ -207,12 +208,9 @@
     b_s[0] = head_out
     b_r[kv] = head_out
 
-    def spread_b(k, carry):
-        peer = ((z + far(k // RING)) % RING) * RING + (y + far(k % RING)) % RING
+    for dz, dy in SPREAD:
+        peer = ((z + dz) % RING) * RING + (y + dy) % RING
         send(b_s.at[0], b_r.at[kv], 6, {"kv": peer, "tp": tp})
-        return carry
-
-    lax.fori_loop(0, 63, spread_b, 0)
     wait_bytes(b_r.at[pl.ds(0, 63)], recv_sem.at[6])
     heads = b_r[...].reshape(128, 512)
     partial = dot_nt(wo_v[...], heads).astype(BF16)
@@ -346,6 +344,17 @@
             wait_bytes(v_r.at[1, pl.ds(0, 1)], send_sem.at[19])
 
 
+def store(mixed_v, state_v, mixed_h, state_h, sem):
+    copies = (
+        pltpu.make_async_copy(state_v, state_h, sem.at[0]),
+        pltpu.make_async_copy(mixed_v, mixed_h, sem.at[1]),
+    )
+    for copy in copies:
+        copy.start()
+    for copy in copies:
+        copy.wait()
+
+
 def local(
     tokens, mix_gain, ffn_gain, w_query, w_key, w_value, w_gate, w_decay, decay_bias, head_gain,
     w_output, w_ffgate, w_ffup, w_down, state,
@@ -355,7 +364,7 @@
     scratch = [
         V((64, 128), BF16), V((1, 64), BF16), V((1, 64), BF16), V((64, 896), BF16), V((64, 896), BF16),
         V((1, 256), F32), V((512,), BF16), V((64, 512), BF16), V((64, hidden_units), BF16),
-        V((64, hidden_units), BF16), V((64, hidden_units), BF16), V((2, 256, 512), F32),
+        V((64, hidden_units), BF16), V((64, hidden_units), BF16),
         V((UNITS, 64, 256), BF16), V((UNITS, 64, 128), BF16),
         V((8, 16, 896), BF16), V((7, 16, 896), BF16), V((8, 16, 896), BF16), V((7, 16, 896), BF16),
         V((8, 2, 896), BF16), V((7, 2, 896), BF16), V((8, 2, 896), BF16), V((7, 2, 896), BF16),
@@ -372,23 +381,30 @@
         tokens.T, mix_gain.reshape(1, 64), ffn_gain.reshape(1, 64), w_query, w_key, w_value, w_gate, w_decay,
         decay_bias.reshape(1, 256), head_gain, w_output.T, w_ffgate, w_ffup, w_down.T, state.reshape(2, 256, 512),
     )
-    mixed, decay, key, value = pl.pallas_call(
+    mixed, new_state = pl.pallas_call(
         kernel,
         name="layer",
         out_shape=(
             jax.ShapeDtypeStruct((64, 128), BF16),
-            jax.ShapeDtypeStruct((2, 256), F32),
-            jax.ShapeDtypeStruct((2, 256), F32),
-            jax.ShapeDtypeStruct((2, 512), F32),
+            jax.ShapeDtypeStruct((2, 256, 512), F32),
         ),
         in_specs=[pl.BlockSpec(memory_space=pltpu.HBM)] * 15,
-        out_specs=[pl.BlockSpec(memory_space=pltpu.VMEM)] * 4,
+        out_specs=[pl.BlockSpec(memory_space=pltpu.VMEM)] * 2,
         scratch_shapes=scratch,
         compiler_params=pltpu.CompilerParams(
             collective_id=0, has_side_effects=True, vmem_limit_bytes=40000000
         ),
     )(*[pltpu.with_memory_space_constraint(a, pltpu.HBM) for a in operands])
-    new_state = decay[:, None, :, None] * state + key[:, None, :, None] * value[:, None, None, :]
+    mixed, new_state = pl.pallas_call(
+        store,
+        name="store",
+        out_shape=(jax.ShapeDtypeStruct((64, 128), BF16), jax.ShapeDtypeStruct((2, 256, 512), F32)),
+        in_specs=[pl.BlockSpec(memory_space=pltpu.VMEM)] * 2,
+        out_specs=[pl.BlockSpec(memory_space=pltpu.HBM)] * 2,
+        scratch_shapes=[pltpu.SemaphoreType.DMA((2,))],
+        compiler_params=pltpu.CompilerParams(vmem_limit_bytes=40000000),
+    )(mixed, new_state)
+    new_state = new_state.reshape(2, 1, 256, 512)
     return (mixed.T, new_state)
 
 

time: 69.4 us -> 68 us (0.980)
  other arithmetic: 1.18 us -> 0 us
    add x1 -> x0, other arithmetic: 1.18 us -> none  [local(): decay[:, None, :, None] * state]
    pallas_call x0 -> x1, Pallas kernels: none -> 0.99 us  [local(): pl.pallas_call(store, name='store', out_shape=(jax.ShapeDtypeStruct((64,...]
where the time goes in v4:
time: 68 us; the launch traced here: 67.8 us
  Pallas kernels  67.2 us (99%)
    pallas_call x1, Pallas kernels, local(): pl.pallas_call(kernel, name='layer', out_shape=(jax.ShapeDtypeStruct((64,...  66.2 us

profile of v4, /device:TPU:1, one launch (start us, length us, event | category | flops | bytes accessed | tf_op | source)
XLA Modules:
  0.0 67.8 jit_solution(10855555228261250159)
XLA Ops:
  0.6 66.2 %layer.1 = (bf16[64,128]{1,0:T(8,128)(2,1)S(1)}, f32[2,256,512]{2,1,0:T(8,128)S(1)}) custom-call(bf16[64,128]{1,0:T(8,128)(2,1)} %bitcast.14, bf16[1,64]{1,0:T(2,128)(2,1)} %bitcast.16, bf16[1,64]{1,0:T(2,128)(2,1)} %bitcast.17, bf16[64,256]{1,0:T(8,128)(2,1)} %wq_h.1, bf16[64,256]{1,0:T(8,128)(2,1)} %wk_h.1, bf16[64,512]{1,0:T(8,128)(2,1)} %wv_h.1, ...), custom_call_target="tpu_custom_call" | custom-call | tf_op jit(solution)/shard_map/layer/pallas_call | solution.py:384
  66.8 1.0 %store.1 = (bf16[64,128]{1,0:T(8,128)(2,1)}, f32[2,256,512]{2,1,0:T(8,128)}) custom-call(bf16[64,128]{1,0:T(8,128)(2,1)S(1)} %get-tuple-element.6.mixed_v, f32[2,256,512]{2,1,0:T(8,128)S(1)} %get-tuple-element.7.state_v), custom_call_target="tpu_custom_call" | custom-call | tf_op jit(solution)/shard_map/store/pallas_call | solution.py:398

commit v5 on v4

--- a/solution.py
+++ b/solution.py
@@ -121,10 +121,10 @@
     ay_s[...] = dot(mix_by_y, w2_v[...]).astype(BF16).reshape(ay_s.shape)
     pl.semaphore_wait(barrier, 21)
     for d in FAR_FIRST:
+        send(ass_s.at[0], ass_r.at[d - 1], 2, at_z(d))
+    for d in FAR_FIRST:
         send(az_s.at[(z + d) % RING], az_r.at[d - 1], 0, at_z(d))
         send(ay_s.at[(y + d) % RING], ay_r.at[d - 1], 1, at_y(d))
-    for d in FAR_FIRST:
-        send(ass_s.at[0], ass_r.at[d - 1], 2, at_z(d))
 
     for copy in copies[8:]:
         copy.wait()
@@ -231,15 +231,22 @@
         attn_out = attn_out + c_r[n].astype(F32)
     mid = (token_f32 + attn_out).astype(BF16).astype(F32)
     ffn_in = (mid * gain_column).astype(BF16)
+    dss_s[0] = square_row(mid)
     x_s[0] = ffn_in
+    for d in FAR_FIRST:
+        send(dss_s.at[0], dss_r.at[d - 1], 11, at_y(d))
+    for d in FAR_FIRST:
+        send(x_s.at[0], x_r.at[y], 10, at_y(d))
     x_r[y] = ffn_in
-    for d in FAR_FIRST:
-        send(x_s.at[0], x_r.at[y], 10, at_y(d))
-    dss_s[0] = square_row(mid)
-    for d in FAR_FIRST:
-        send(dss_s.at[0], dss_r.at[d - 1], 11, at_y(d))
 
     second = y % 3 == 0
+    wait_bytes(dss_r, recv_sem.at[11])
+    ss = dss_s[0]
+    for n in range(7):
+        ss = ss + dss_r[n]
+    dss2_s[0] = ss
+    for d in FAR_FIRST:
+        send(dss2_s.at[0], dss2_r.at[d - 1], 14, at_z(d))
     wait_bytes(w_r.at[0, pl.ds(0, 7)], recv_sem.at[8])
     wait_bytes(x_r.at[pl.ds(0, 7)], recv_sem.at[10])
     rows_in = dot_nt(keep, x_r[...].reshape(512, 128)).astype(BF16)
@@ -261,13 +268,6 @@
         def _(d=d):
             send(wdt_v.at[8 + (y + d) % RING // 3], v_r.at[1, y], 19, at_y(d))
 
-    wait_bytes(dss_r, recv_sem.at[11])
-    ss = dss_s[0]
-    for n in range(7):
-        ss = ss + dss_r[n]
-    dss2_s[0] = ss
-    for d in FAR_FIRST:
-        send(dss2_s.at[0], dss2_r.at[d - 1], 14, at_z(d))
     wait_bytes(dss2_r, recv_sem.at[14])
     for n in range(7):
         ss = ss + dss2_r[n]

time: 68 us -> 67 us (0.985)
  Pallas kernels: 67.2 us -> 66.2 us
    pallas_call x1, Pallas kernels: 66.2 us -> 65.2 us  [local(): pl.pallas_call(kernel, name='layer', out_shape=(jax.ShapeDtypeStruct((64,...]
where the time goes in v5:
time: 67 us; the launch traced here: 66.8 us
  Pallas kernels  66.2 us (99%)
    pallas_call x1, Pallas kernels, local(): pl.pallas_call(kernel, name='layer', out_shape=(jax.ShapeDtypeStruct((64,...  65.2 us

profile of v5, /device:TPU:1, one launch (start us, length us, event | category | flops | bytes accessed | tf_op | source)
XLA Modules:
  0.0 66.8 jit_solution(9364764058306501110)
XLA Ops:
  0.6 65.2 %layer.1 = (bf16[64,128]{1,0:T(8,128)(2,1)S(1)}, f32[2,256,512]{2,1,0:T(8,128)S(1)}) custom-call(bf16[64,128]{1,0:T(8,128)(2,1)} %bitcast.14, bf16[1,64]{1,0:T(2,128)(2,1)} %bitcast.16, bf16[1,64]{1,0:T(2,128)(2,1)} %bitcast.17, bf16[64,256]{1,0:T(8,128)(2,1)} %wq_h.1, bf16[64,256]{1,0:T(8,128)(2,1)} %wk_h.1, bf16[64,512]{1,0:T(8,128)(2,1)} %wv_h.1, ...), custom_call_target="tpu_custom_call" | custom-call | tf_op jit(solution)/shard_map/layer/pallas_call | solution.py:384
  65.8 1.0 %store.1 = (bf16[64,128]{1,0:T(8,128)(2,1)}, f32[2,256,512]{2,1,0:T(8,128)}) custom-call(bf16[64,128]{1,0:T(8,128)(2,1)S(1)} %get-tuple-element.6.mixed_v, f32[2,256,512]{2,1,0:T(8,128)S(1)} %get-tuple-element.7.state_v), custom_call_target="tpu_custom_call" | custom-call | tf_op jit(solution)/shard_map/store/pallas_call | solution.py:398
